TPU v7x, 32 devices: a whole 2x2x4 slice. The times are simulated.
32 devices in a mesh: sp: 16 (over z, y, x), tp: 2 (over core).
Axes of the slice: x: 2, y: 2, z: 4, core: 2. Of those that a mesh axis runs over, the one named last changes fastest.
Arguments:
- queries: bfloat16 [4096, 1024], P('sp', 'tp'), may hold values from -12 to 12
- keys: bfloat16 [4096, 1024], P('sp', 'tp'), may hold values from -6 to 6
- values: bfloat16 [4096, 1024], P('sp', 'tp'), may hold values from -6 to 6
- w_out: bfloat16 [1024, 2048], P(None, 'tp'), may hold values from -0.375 to 0.375
Outputs:
- mixed: bfloat16 [4096, 2048], P('sp', 'tp')
All inputs are finite; a program needn't handle non-finite values.
Results may differ from a plain program's by a relative error of at most 0.0056.
Values may be sent and summed in bfloat16 or wider, within the bound.
No kernel may reach another device: no remote copies, remote signals or barrier semaphores. Data moves between devices by JAX's collectives and lax.ppermute only.
A program may use at most 64 MiB of HBM per device.

v0:
```python
import jax
import jax.numpy as jnp
from jax import lax
from jax.sharding import PartitionSpec as P

HEAD_DIM = 128
SIDE_KEY_COUNT = 64
MIDDLE_DILATION = 4
FAR_DILATION = 16


def from_behind(value, axis, steps):
    count = lax.axis_size(axis)
    first, last = (max(0, -steps), min(count, count - steps))
    return lax.ppermute(value, axis, [(source, source + steps) for source in range(first, last)])


def band_scores(queries, window_keys, start_position, sequence_length, dilation_step):
    nearby_rows, columns = queries.shape
    heads = columns // HEAD_DIM
    residue_rows = nearby_rows // dilation_step
    blocks = residue_rows // residue_rows
    span = residue_rows + 2 * SIDE_KEY_COUNT
    laid = jnp.transpose(
        window_keys.reshape(2, residue_rows + 2 * SIDE_KEY_COUNT, dilation_step, heads, HEAD_DIM),
        (0, 2, 3, 1, 4),
    )
    grouped = jnp.transpose(
        queries.reshape(blocks, residue_rows, dilation_step, heads, HEAD_DIM), (0, 2, 3, 1, 4)
    )
    query_idx = jnp.arange(residue_rows, dtype=jnp.int32)[:, None]
    key_idx = jnp.arange(span, dtype=jnp.int32)[None, :]
    in_band = (key_idx >= query_idx) & (key_idx <= query_idx + 2 * SIDE_KEY_COUNT)
    residues = jnp.arange(dilation_step, dtype=jnp.int32)[:, None, None, None]
    scale = HEAD_DIM ** (-0.5)

    def one_block(inputs):
        number, query_block = inputs
        first_row = number * residue_rows
        scores = (
            jnp.einsum("rhqe,rhke->rhqk", query_block, laid[0], preferred_element_type=jnp.float32)
            * scale
        )
        key_pos = (
            start_position
            + (first_row + key_idx[None, None] - SIDE_KEY_COUNT) * dilation_step
            + residues
        )
        allowed = in_band[None, None] & (key_pos >= 0) & (key_pos < sequence_length)
        scores = jnp.where(allowed, scores, -jnp.inf)
        maximum = jnp.max(scores, axis=-1, keepdims=True)
        raised = jnp.exp(scores - maximum)
        denominator = jnp.sum(raised, axis=-1, keepdims=True)
        weights = (raised / denominator).astype(jnp.bfloat16)
        attended = jnp.einsum(
            "rhqk,rhke->rhqe", weights, laid[1], preferred_element_type=jnp.float32
        )
        log_den = (maximum + jnp.log(denominator))[..., 0]
        return (attended, log_den)

    outputs, log_dens = lax.map(one_block, (jnp.arange(blocks, dtype=jnp.int32), grouped))
    attended = jnp.transpose(outputs, (0, 3, 1, 2, 4)).reshape(nearby_rows, heads, HEAD_DIM)
    log_den = jnp.transpose(log_dens, (0, 3, 1, 2)).reshape(nearby_rows, heads)
    return (attended, log_den)


def far_blocks(stacked_groups, hop_count):
    offsets = list(range(hop_count, 0, -1)) + list(range(-1, -hop_count - 1, -1))
    moved = [from_behind(stacked_groups, "sp", offset) for offset in offsets]
    return moved[:hop_count] + [stacked_groups] + moved[hop_count:]


def per_device(queries, keys, values, w_out):
    nearby_rows, columns = queries.shape
    sequence_length = nearby_rows * lax.axis_size("sp")
    start_position = lax.axis_index("sp") * nearby_rows
    stacked_groups = jnp.stack([keys, values])
    hop_count = -(-(SIDE_KEY_COUNT * FAR_DILATION) // nearby_rows)
    extended = jnp.concatenate(far_blocks(stacked_groups, hop_count), axis=1)

    def window_keys(dilation_step):
        padding = SIDE_KEY_COUNT * dilation_step
        return lax.slice_in_dim(
            extended,
            hop_count * nearby_rows - padding,
            (hop_count + 1) * nearby_rows + padding,
            axis=1,
        )

    nearby = window_keys(1)
    middle_group = window_keys(MIDDLE_DILATION)
    distant_group = window_keys(FAR_DILATION)
    group_results = [
        band_scores(queries, nearby, start_position, sequence_length, 1),
        band_scores(queries, middle_group, start_position, sequence_length, MIDDLE_DILATION),
        band_scores(queries, distant_group, start_position, sequence_length, FAR_DILATION),
    ]
    stacked_out = jnp.stack([item[0] for item in group_results])
    stacked_den = jnp.stack([item[1] for item in group_results])
    shares = jax.nn.softmax(stacked_den, axis=0)
    attended = (
        jnp.sum(shares[..., None] * stacked_out, axis=0)
        .astype(jnp.bfloat16)
        .reshape(nearby_rows, columns)
    )
    mixed = jnp.dot(
        lax.all_gather(attended, "tp", axis=1, tiled=True),
        w_out,
        preferred_element_type=jnp.float32,
    )
    return mixed.astype(jnp.bfloat16)


def solution(mesh):
    in_specs = (P("sp", "tp"), P("sp", "tp"), P("sp", "tp"), P(None, "tp"))
    out_specs = P("sp", "tp")
    return jax.shard_map(
        per_device, mesh=mesh, in_specs=in_specs, out_specs=out_specs, check_vma=False
    )
```

profile of v0, /device:TPU:17, one launch (start us, length us, event | category | flops | bytes accessed | tf_op | source)
XLA Modules:
  0.0 139.6 jit_solution(15422659111726366971)
XLA Ops:
  0.0 1.2 copy.49
  1.2 1.1 copy.50
  2.3 0.8 pad_maximum_fusion.1
  3.2 3.2 %collective-permute-start.2 = (bf16[2,256,512]{1,2,0:T(8,128)(2,1)}, bf16[2,256,512]{1,2,0:T(8,128)(2,1)}, u32[]{:S(2)}, u32[]{:S(2)}) collective-permute-start(bf16[2,256,512]{1,2,0:T(8,128)(2,1)} %pad_maximum_fusion.1), channel_id=1, source_target_pairs={{0,8},{2,10},{4,12},{6,14},{8,16},{10,18},{12,20},{14,22},{16,24},... | collective-permute-start | bytes 1572872 | tf_op jit(solution)/shard_map/ppermute | solution.py:15
  6.4 4.1 %collective-permute-start.3 = (bf16[2,256,512]{1,2,0:T(8,128)(2,1)}, bf16[2,256,512]{1,2,0:T(8,128)(2,1)}, u32[]{:S(2)}, u32[]{:S(2)}) collective-permute-start(bf16[2,256,512]{1,2,0:T(8,128)(2,1)} %pad_maximum_fusion.1), channel_id=1, source_target_pairs={{0,6},{2,8},{4,10},{6,12},{8,14},{10,16},{12,18},{14,20},{16,22},{... | collective-permute-start | bytes 1572872 | tf_op jit(solution)/shard_map/ppermute | solution.py:15
  10.5 1.9 %collective-permute-start.4 = (bf16[2,256,512]{1,2,0:T(8,128)(2,1)}, bf16[2,256,512]{1,2,0:T(8,128)(2,1)}, u32[]{:S(2)}, u32[]{:S(2)}) collective-permute-start(bf16[2,256,512]{1,2,0:T(8,128)(2,1)} %pad_maximum_fusion.1), channel_id=1, source_target_pairs={{0,4},{2,6},{4,8},{6,10},{8,12},{10,14},{12,16},{14,18},{16,20},{1... | collective-permute-start | bytes 1572872 | tf_op jit(solution)/shard_map/ppermute | solution.py:15
  12.4 2.2 %collective-permute-start = (bf16[2,256,512]{1,2,0:T(8,128)(2,1)}, bf16[2,256,512]{1,2,0:T(8,128)(2,1)}, u32[]{:S(2)}, u32[]{:S(2)}) collective-permute-start(bf16[2,256,512]{1,2,0:T(8,128)(2,1)} %pad_maximum_fusion.1), channel_id=1, source_target_pairs={{0,2},{2,4},{4,6},{6,8},{8,10},{10,12},{12,14},{14,16},{16,18},{18... | collective-permute-start | bytes 1572872 | tf_op jit(solution)/shard_map/ppermute | solution.py:15
  14.6 4.9 %collective-permute-start.1 = (bf16[2,256,512]{1,2,0:T(8,128)(2,1)}, bf16[2,256,512]{1,2,0:T(8,128)(2,1)S(1)}, u32[]{:S(2)}, u32[]{:S(2)}) collective-permute-start(bf16[2,256,512]{1,2,0:T(8,128)(2,1)} %pad_maximum_fusion.1), channel_id=1, source_target_pairs={{2,0},{4,2},{6,4},{8,6},{10,8},{12,10},{14,12},{16,14},{18,16},{20... | collective-permute-start | bytes 1572872 | tf_op jit(solution)/shard_map/ppermute | solution.py:15
  19.6 0.1 fusion.25
  19.7 0.7 and_and_fusion.1
  20.3 0.8 fusion.18
  21.1 0.1 fusion.27
  21.2 0.8 reshape.466
  22.0 0.8 reshape.464
  22.8 0.8 reshape.461
  23.6 3.4 %collective-permute-start.5 = (bf16[2,256,512]{1,2,0:T(8,128)(2,1)}, bf16[2,256,512]{1,2,0:T(8,128)(2,1)}, u32[]{:S(2)}, u32[]{:S(2)}) collective-permute-start(bf16[2,256,512]{1,2,0:T(8,128)(2,1)} %pad_maximum_fusion.1), channel_id=1, source_target_pairs={{4,0},{6,2},{8,4},{10,6},{12,8},{14,10},{16,12},{18,14},{20,16},{2... | collective-permute-start | bytes 1572872 | tf_op jit(solution)/shard_map/ppermute | solution.py:15
  27.0 1.9 %constant_dynamic-update-slice_fusion.8 = bf16[2,2304,512]{1,2,0:T(8,128)(2,1)} fusion(bf16[2,256,512]{1,2,0:T(8,128)(2,1)} %collective-permute-done.2), kind=kLoop, calls=%fused_computation.63 | loop fusion | bytes 1048576
  28.9 27.7 %collective-permute-done = bf16[2,256,512]{1,2,0:T(8,128)(2,1)} collective-permute-done((bf16[2,256,512]{1,2,0:T(8,128)(2,1)}, bf16[2,256,512]{1,2,0:T(8,128)(2,1)}, u32[]{:S(2)}, u32[]{:S(2)}) %collective-permute-start) | collective-permute-done | bytes 524320 | tf_op jit(solution)/shard_map/ppermute | solution.py:15
  56.6 1.9 %collective-permute-start.6 = (bf16[2,256,512]{1,2,0:T(8,128)(2,1)}, bf16[2,256,512]{1,2,0:T(8,128)(2,1)}, u32[]{:S(2)}, u32[]{:S(2)}) collective-permute-start(bf16[2,256,512]{1,2,0:T(8,128)(2,1)} %pad_maximum_fusion.1), channel_id=1, source_target_pairs={{6,0},{8,2},{10,4},{12,6},{14,8},{16,10},{18,12},{20,14},{22,16},{... | collective-permute-start | bytes 1572872 | tf_op jit(solution)/shard_map/ppermute | solution.py:15
  58.6 7.2 %collective-permute-done.1 = bf16[2,256,512]{1,2,0:T(8,128)(2,1)S(1)} collective-permute-done((bf16[2,256,512]{1,2,0:T(8,128)(2,1)}, bf16[2,256,512]{1,2,0:T(8,128)(2,1)S(1)}, u32[]{:S(2)}, u32[]{:S(2)}) %collective-permute-start.1) | collective-permute-done | bytes 524320 | tf_op jit(solution)/shard_map/ppermute | solution.py:15
  65.8 5.1 %collective-permute-start.7 = (bf16[2,256,512]{1,2,0:T(8,128)(2,1)}, bf16[2,256,512]{1,2,0:T(8,128)(2,1)}, u32[]{:S(2)}, u32[]{:S(2)}) collective-permute-start(bf16[2,256,512]{1,2,0:T(8,128)(2,1)} %pad_maximum_fusion.1), channel_id=1, source_target_pairs={{8,0},{10,2},{12,4},{14,6},{16,8},{18,10},{20,12},{22,14},{24,16},... | collective-permute-start | bytes 1572872 | tf_op jit(solution)/shard_map/ppermute | solution.py:15
  70.8 2.3 %pad_maximum_fusion = bf16[2,768,512]{1,2,0:T(8,128)(2,1)} fusion(bf16[2,256,512]{1,2,0:T(8,128)(2,1)S(1)} %collective-permute-done.1, bf16[1,256,512]{1,2,0:T(8,128)(2,1)S(1)} %bitcast.133, bf16[1,256,512]{1,2,0:T(8,128)(2,1)S(1)} %bitcast.130, bf16[2,256,512]{1,2,0:T(8,128)(2,1)} %collective-permute-done), kind=kLoop, calls=%fused_computation.5 | loop fusion | flops 6291456 | bytes 3145728 | tf_op jit(solution)/shard_map/concatenate | solution.py:79
  73.2 1.9 %constant_dynamic-update-slice_fusion.7 = bf16[2,2304,512]{1,2,0:T(8,128)(2,1)} fusion(bf16[2,2304,512]{1,2,0:T(8,128)(2,1)} %constant_dynamic-update-slice_fusion.8, bf16[2,256,512]{1,2,0:T(8,128)(2,1)} %collective-permute-done.3), kind=kLoop, calls=%fused_computation.62 | loop fusion | bytes 1048576
  75.1 1.9 %constant_dynamic-update-slice_fusion.6 = bf16[2,2304,512]{1,2,0:T(8,128)(2,1)} fusion(bf16[2,2304,512]{1,2,0:T(8,128)(2,1)} %constant_dynamic-update-slice_fusion.7, bf16[2,256,512]{1,2,0:T(8,128)(2,1)} %collective-permute-done.4), kind=kLoop, calls=%fused_computation.61 | loop fusion | bytes 1048576
  77.0 1.9 %constant_dynamic-update-slice_fusion.5 = bf16[2,2304,512]{1,2,0:T(8,128)(2,1)} fusion(bf16[2,2304,512]{1,2,0:T(8,128)(2,1)} %constant_dynamic-update-slice_fusion.6, bf16[2,256,512]{1,2,0:T(8,128)(2,1)} %collective-permute-done), kind=kLoop, calls=%fused_computation.60 | loop fusion | bytes 1048576
  78.9 2.6 %copy.53 = bf16[2,768,512]{2,1,0:T(8,128)(2,1)} copy(bf16[2,768,512]{1,2,0:T(8,128)(2,1)} %pad_maximum_fusion) | data formatting | bytes 3145728 | tf_op jit(solution)/shard_map/concatenate | solution.py:79
  81.6 1.6 %slice.37 = bf16[2,384,512]{1,2,0:T(8,128)(2,1)S(1)} slice(bf16[2,768,512]{1,2,0:T(8,128)(2,1)} %pad_maximum_fusion), slice={[0:2], [192:576], [0:512]} | slice | bytes 1572864 | tf_op jit(solution)/shard_map/slice | solution.py:83
  83.2 0.9 constant_dynamic-update-slice_fusion.4
  84.0 0.9 constant_dynamic-update-slice_fusion.3
  84.9 1.9 %constant_dynamic-update-slice_fusion.2 = bf16[2,2304,512]{1,2,0:T(8,128)(2,1)} fusion(bf16[2,2304,512]{1,2,0:T(8,128)(2,1)} %constant_dynamic-update-slice_fusion.3, bf16[2,256,512]{1,2,0:T(8,128)(2,1)} %collective-permute-done.5), kind=kLoop, calls=%fused_computation.57 | loop fusion | bytes 1048576
  86.8 1.9 %constant_dynamic-update-slice_fusion.1 = bf16[2,2304,512]{1,2,0:T(8,128)(2,1)} fusion(bf16[2,2304,512]{1,2,0:T(8,128)(2,1)} %constant_dynamic-update-slice_fusion.2, bf16[2,256,512]{1,2,0:T(8,128)(2,1)} %collective-permute-done.6), kind=kLoop, calls=%fused_computation.56 | loop fusion | bytes 1048576
  88.7 1.9 %constant_dynamic-update-slice_fusion = bf16[2,2304,512]{1,2,0:T(8,128)(2,1)} fusion(bf16[2,2304,512]{1,2,0:T(8,128)(2,1)} %constant_dynamic-update-slice_fusion.1, bf16[2,256,512]{1,2,0:T(8,128)(2,1)} %collective-permute-done.7), kind=kLoop, calls=%fused_computation.55 | loop fusion | bytes 1048576 | tf_op jit(solution)/shard_map/concatenate | solution.py:79
  90.6 6.7 %copy.57 = bf16[2,2304,512]{2,1,0:T(8,128)(2,1)} copy(bf16[2,2304,512]{1,2,0:T(8,128)(2,1)} %constant_dynamic-update-slice_fusion) | data formatting | bytes 9437184 | tf_op jit(solution)/shard_map/concatenate | solution.py:79
  97.3 7.7 %reshape.465 = bf16[2,144,16,4,128]{4,3,2,1,0:T(4,128)(2,1)} reshape(bf16[2,2304,512]{2,1,0:T(8,128)(2,1)} %copy.57) | data formatting | bytes 9437184 | tf_op jit(solution)/shard_map/reshape | solution.py:25
  105.0 7.8 %copy.88 = bf16[2,144,16,4,128]{4,1,3,2,0:T(8,128)(2,1)S(1)} copy(bf16[2,144,16,4,128]{4,3,2,1,0:T(4,128)(2,1)} %reshape.465) | data formatting | bytes 9437184 | tf_op jit(solution)/shard_map/reshape | solution.py:25
  112.9 1.4 %fusion.37 = (f32[16,4,16]{2,1,0:T(4,128)S(1)}, f32[16,4,16,144]{3,2,1,0:T(8,128)S(1)}) fusion(bf16[1,16,16,4,128]{4,3,2,1,0:T(4,128)(2,1)S(1)} %copy-done.13, bf16[2,16,4,144,128]{4,3,2,1,0:T(8,128)(2,1)S(1)} %bitcast.127, pred[16,16,144]{2,1,0:T(8,128)(4,1)S(1)} %and_and_fusion), kind=kOutput, calls=%fused_computation.90 | convolution fusion | flops 38190080 | bytes 3280896 | tf_op jit(solution)/shard_map/while/body/eval_jaxpr/rhqe,rhke->rhqk/dot_general | solution.py:41
  114.3 0.7 copy-done.1
  115.1 1.0 copy-done.7
  116.0 0.4 fusion.11
  116.5 0.1 copy.60
  116.6 0.1 stack_reshape.20
  116.7 0.1 stack.26
  116.8 3.5 %reshape.463 = bf16[2,192,4,4,128]{4,3,2,1,0:T(4,128)(2,1)} reshape(bf16[2,768,512]{2,1,0:T(8,128)(2,1)} %copy.53) | data formatting | bytes 3145728 | tf_op jit(solution)/shard_map/reshape | solution.py:25
  120.3 1.9 %copy.89 = bf16[2,192,4,4,128]{4,1,3,2,0:T(8,128)(2,1)S(1)} copy(bf16[2,192,4,4,128]{4,3,2,1,0:T(4,128)(2,1)} %reshape.463) | data formatting | bytes 3145728 | tf_op jit(solution)/shard_map/reshape | solution.py:25
  122.1 1.2 copy-done.5
  123.3 0.7 fusion.38
  124.0 0.4 fusion.10
  124.5 0.6 copy-done.8
  125.1 0.1 copy.56
  125.2 0.1 stack_reshape.19
  125.4 0.1 stack.25
  125.5 2.9 %fusion.9 = f32[1,16,16,4,128]{4,1,3,2,0:T(8,128)S(1)} fusion(bf16[2,16,4,144,128]{4,3,2,1,0:T(8,128)(2,1)} %bitcast.128, f32[16,4,16,144]{3,2,1,0:T(8,128)} %copy-done.7, f32[16,4,16]{2,1,0:T(4,128)S(1)} %fusion.11, f32[16,4,16]{2,1,0:T(4,128)S(1)} %get-tuple-element.58), kind=kOutput, calls=%fused_computation.22 | convolution fusion | flops 38191104 | bytes 3940352 | tf_op jit(solution)/shard_map/while/body/eval_jaxpr/rhqk,rhke->rhqe/dot_general | solution.py:55
  128.5 1.3 convolution_bitcast_fusion
  129.7 1.2 copy.51
  130.9 1.5 %fusion.39 = (f32[4,256]{1,0:T(4,128)S(1)}, f32[4,256,384]{1,2,0:T(8,128)S(1)}) fusion(bf16[1,256,1,4,128]{4,3,1,2,0:T(4,128)(2,1)} %reshape.461, bf16[2,1,4,384,128]{4,3,2,1,0:T(8,128)(2,1)} %bitcast.141, pred[256,384]{0,1:T(8,128)(4,1)S(1)} %copy-done.14), kind=kOutput, calls=%fused_computation.92 | convolution fusion | flops 101841920 | bytes 2330624 | tf_op jit(solution)/shard_map/while/body/eval_jaxpr/rhqe,rhke->rhqk/dot_general | solution.py:41
  132.4 0.2 fusion.3
  132.7 0.5 convolution_bitcast_fusion.1
  133.3 0.3 copy.65
  133.6 0.1 copy-done.11
  133.7 0.3 copy.64
  134.1 0.5 fusion.2
  134.6 0.1 copy.66
  134.7 3.4 %all_gather.3 = bf16[256,1024]{0,1:T(8,128)(2,1)S(1)} all-gather(bf16[256,512]{0,1:T(8,128)(2,1)S(1)} %bitcast.140), channel_id=1, replica_groups=mesh['sp'=16,'tp'=2] {'tp'}, dimensions={1}, use_global_device_ids=true | all-gather | bytes 786432 | tf_op jit(solution)/shard_map/all_gather | solution.py:107
  138.1 1.5 %convolution_convert_fusion = bf16[256,1024]{1,0:T(8,128)(2,1)} fusion(bf16[256,1024]{0,1:T(8,128)(2,1)S(1)} %all_gather.3, bf16[1024,1024]{1,0:T(8,128)(2,1)S(1)} %copy-done), kind=kOutput, calls=%fused_computation.19 | convolution fusion | flops 537133056 | bytes 3145728 | tf_op jit(solution)/shard_map/dot_general | solution.py:106
  (47 shorter events, 0.2 us)
Async XLA Ops:
  0.0 138.1 %copy-start = (bf16[1024,1024]{1,0:T(8,128)(2,1)S(1)}, bf16[1024,1024]{1,0:T(8,128)(2,1)}, u32[]{:S(2)}) copy-start(bf16[1024,1024]{1,0:T(8,128)(2,1)} %param.7) | copy-start | bytes 6291460
  0.0 21.2 %copy-start.2 = (bf16[256,512]{1,0:T(8,128)(2,1)S(1)}, bf16[256,512]{1,0:T(8,128)(2,1)}, u32[]{:S(2)}) copy-start(bf16[256,512]{1,0:T(8,128)(2,1)} %param.4) | copy-start | bytes 786436
  3.2 20.4 %collective-permute-start.2 = (bf16[2,256,512]{1,2,0:T(8,128)(2,1)}, bf16[2,256,512]{1,2,0:T(8,128)(2,1)}, u32[]{:S(2)}, u32[]{:S(2)}) collective-permute-start(bf16[2,256,512]{1,2,0:T(8,128)(2,1)} %pad_maximum_fusion.1), channel_id=1, source_target_pairs={{0,8},{2,10},{4,12},{6,14},{8,16},{10,18},{12,20},{14,22},{16,24},... | collective-permute-start | bytes 1572872 | tf_op jit(solution)/shard_map/ppermute | solution.py:15
  6.4 66.8 %collective-permute-start.3 = (bf16[2,256,512]{1,2,0:T(8,128)(2,1)}, bf16[2,256,512]{1,2,0:T(8,128)(2,1)}, u32[]{:S(2)}, u32[]{:S(2)}) collective-permute-start(bf16[2,256,512]{1,2,0:T(8,128)(2,1)} %pad_maximum_fusion.1), channel_id=1, source_target_pairs={{0,6},{2,8},{4,10},{6,12},{8,14},{10,16},{12,18},{14,20},{16,22},{... | collective-permute-start | bytes 1572872 | tf_op jit(solution)/shard_map/ppermute | solution.py:15
  10.5 64.6 %collective-permute-start.4 = (bf16[2,256,512]{1,2,0:T(8,128)(2,1)}, bf16[2,256,512]{1,2,0:T(8,128)(2,1)}, u32[]{:S(2)}, u32[]{:S(2)}) collective-permute-start(bf16[2,256,512]{1,2,0:T(8,128)(2,1)} %pad_maximum_fusion.1), channel_id=1, source_target_pairs={{0,4},{2,6},{4,8},{6,10},{8,12},{10,14},{12,16},{14,18},{16,20},{1... | collective-permute-start | bytes 1572872 | tf_op jit(solution)/shard_map/ppermute | solution.py:15
  12.4 44.2 %collective-permute-start = (bf16[2,256,512]{1,2,0:T(8,128)(2,1)}, bf16[2,256,512]{1,2,0:T(8,128)(2,1)}, u32[]{:S(2)}, u32[]{:S(2)}) collective-permute-start(bf16[2,256,512]{1,2,0:T(8,128)(2,1)} %pad_maximum_fusion.1), channel_id=1, source_target_pairs={{0,2},{2,4},{4,6},{6,8},{8,10},{10,12},{12,14},{14,16},{16,18},{18... | collective-permute-start | bytes 1572872 | tf_op jit(solution)/shard_map/ppermute | solution.py:15
  14.6 51.2 %collective-permute-start.1 = (bf16[2,256,512]{1,2,0:T(8,128)(2,1)}, bf16[2,256,512]{1,2,0:T(8,128)(2,1)S(1)}, u32[]{:S(2)}, u32[]{:S(2)}) collective-permute-start(bf16[2,256,512]{1,2,0:T(8,128)(2,1)} %pad_maximum_fusion.1), channel_id=1, source_target_pairs={{2,0},{4,2},{6,4},{8,6},{10,8},{12,10},{14,12},{16,14},{18,16},{20... | collective-permute-start | bytes 1572872 | tf_op jit(solution)/shard_map/ppermute | solution.py:15
  23.6 61.3 %collective-permute-start.5 = (bf16[2,256,512]{1,2,0:T(8,128)(2,1)}, bf16[2,256,512]{1,2,0:T(8,128)(2,1)}, u32[]{:S(2)}, u32[]{:S(2)}) collective-permute-start(bf16[2,256,512]{1,2,0:T(8,128)(2,1)} %pad_maximum_fusion.1), channel_id=1, source_target_pairs={{4,0},{6,2},{8,4},{10,6},{12,8},{14,10},{16,12},{18,14},{20,16},{2... | collective-permute-start | bytes 1572872 | tf_op jit(solution)/shard_map/ppermute | solution.py:15
  56.6 30.2 %collective-permute-start.6 = (bf16[2,256,512]{1,2,0:T(8,128)(2,1)}, bf16[2,256,512]{1,2,0:T(8,128)(2,1)}, u32[]{:S(2)}, u32[]{:S(2)}) collective-permute-start(bf16[2,256,512]{1,2,0:T(8,128)(2,1)} %pad_maximum_fusion.1), channel_id=1, source_target_pairs={{6,0},{8,2},{10,4},{12,6},{14,8},{16,10},{18,12},{20,14},{22,16},{... | collective-permute-start | bytes 1572872 | tf_op jit(solution)/shard_map/ppermute | solution.py:15
  65.8 11.3 %copy-start.3 = (bf16[2,256,512]{1,2,0:T(8,128)(2,1)}, bf16[2,256,512]{1,2,0:T(8,128)(2,1)S(1)}, u32[]{:S(2)}) copy-start(bf16[2,256,512]{1,2,0:T(8,128)(2,1)S(1)} %collective-permute-done.1) | copy-start | bytes 1572868
  65.8 23.0 %collective-permute-start.7 = (bf16[2,256,512]{1,2,0:T(8,128)(2,1)}, bf16[2,256,512]{1,2,0:T(8,128)(2,1)}, u32[]{:S(2)}, u32[]{:S(2)}) collective-permute-start(bf16[2,256,512]{1,2,0:T(8,128)(2,1)} %pad_maximum_fusion.1), channel_id=1, source_target_pairs={{8,0},{10,2},{12,4},{14,6},{16,8},{18,10},{20,12},{22,14},{24,16},... | collective-permute-start | bytes 1572872 | tf_op jit(solution)/shard_map/ppermute | solution.py:15
  81.6 2.5 %copy-start.4 = (bf16[2,256,512]{1,2,0:T(8,128)(2,1)S(1)}, bf16[2,256,512]{1,2,0:T(8,128)(2,1)}, u32[]{:S(2)}) copy-start(bf16[2,256,512]{1,2,0:T(8,128)(2,1)} %copy-done.3) | copy-start | bytes 1572868
  105.0 7.9 %copy-start.13 = (bf16[1,16,16,4,128]{4,3,2,1,0:T(4,128)(2,1)S(1)}, bf16[1,16,16,4,128]{4,3,2,1,0:T(4,128)(2,1)}, u32[]{:S(2)}) copy-start(bf16[1,16,16,4,128]{4,3,2,1,0:T(4,128)(2,1)} %reshape.466) | copy-start | bytes 786436
  112.9 2.2 %copy-start.1 = (bf16[2,144,16,4,128]{4,1,3,2,0:T(8,128)(2,1)}, bf16[2,144,16,4,128]{4,1,3,2,0:T(8,128)(2,1)S(1)}, u32[]{:S(2)}) copy-start(bf16[2,144,16,4,128]{4,1,3,2,0:T(8,128)(2,1)S(1)} %copy.88) | copy-start | bytes 14155780
  115.1 1.0 copy-start.7
  120.3 3.1 %copy-start.12 = (bf16[1,64,4,4,128]{4,3,2,1,0:T(4,128)(2,1)S(1)}, bf16[1,64,4,4,128]{4,3,2,1,0:T(4,128)(2,1)}, u32[]{:S(2)}) copy-start(bf16[1,64,4,4,128]{4,3,2,1,0:T(4,128)(2,1)} %reshape.464) | copy-start | bytes 786436
  120.3 3.1 %copy-start.15 = (pred[4,64,192]{2,1,0:T(8,128)(4,1)S(1)}, pred[4,64,192]{2,1,0:T(8,128)(4,1)}, u32[]{:S(2)}) copy-start(pred[4,64,192]{2,1,0:T(8,128)(4,1)} %and_and_fusion.1) | copy-start | bytes 147460
  122.1 1.2 copy-start.5
  124.0 1.1 copy-start.8
  125.5 2.9 %copy-start.6 = (bf16[2,192,4,4,128]{4,1,3,2,0:T(8,128)(2,1)S(1)}, bf16[2,192,4,4,128]{4,1,3,2,0:T(8,128)(2,1)}, u32[]{:S(2)}) copy-start(bf16[2,192,4,4,128]{4,1,3,2,0:T(8,128)(2,1)} %copy-done.5) | copy-start | bytes 4718596
  125.5 2.9 %copy-start.9 = (f32[4,4,64,192]{3,2,1,0:T(8,128)S(1)}, f32[4,4,64,192]{3,2,1,0:T(8,128)}, u32[]{:S(2)}) copy-start(f32[4,4,64,192]{3,2,1,0:T(8,128)} %copy-done.8) | copy-start | bytes 2359300
  128.4 2.5 %copy-start.14 = (pred[256,384]{0,1:T(8,128)(4,1)S(1)}, pred[256,384]{0,1:T(8,128)(4,1)}, u32[]{:S(2)}) copy-start(pred[256,384]{0,1:T(8,128)(4,1)} %fusion.18) | copy-start | bytes 294916
  130.9 1.8 %copy-start.10 = (bf16[2,384,1,4,128]{4,1,3,2,0:T(8,128)(2,1)S(1)}, bf16[2,384,1,4,128]{4,1,3,2,0:T(8,128)(2,1)}, u32[]{:S(2)}) copy-start(bf16[2,384,1,4,128]{4,1,3,2,0:T(8,128)(2,1)} %copy.51) | copy-start | bytes 2359300
  132.7 1.0 copy-start.11
where the time goes:
time: 141 us; the launch traced here: 140 us
  local copies, waits for them, and re-layouts  57 us (40%)
  waiting for transfers between devices  35 us (25%)
  starting transfers between devices  26.6 us (19%)
  matrix products  9.89 us (7%)
  other arithmetic  7.38 us (5%)
  blocking collectives  3.41 us (2%)
    ppermute x8, waiting for transfers between devices, from_behind(): lax.ppermute(value, axis, [(source, source + steps) for source in range(f...  35 us
    ppermute x8, starting transfers between devices, from_behind(): lax.ppermute(value, axis, [(source, source + steps) for source in range(f...  26.6 us
    reshape x5, local copies, waits for them, and re-layouts, band_scores(): window_keys.reshape(2, residue_rows + 2 * SIDE_KEY_COUNT, dilation_step,...  22.1 us
    unnamed x41, local copies, waits for them, and re-layouts  18.4 us
    concatenate x3, local copies, waits for them, and re-layouts, per_device(): extended = jnp.concatenate(far_blocks(stacked_groups, hop_count), axis=1)  11.2 us
    dot_general x3, matrix products, one_block(): jnp.einsum('rhqk,rhke->rhqe', weights, laid[1], preferred_element_type=jn...  4.69 us
    dot_general x3, matrix products, one_block(): jnp.einsum('rhqe,rhke->rhqk', query_block, laid[0], preferred_element_typ...  3.68 us
    all_gather x1, blocking collectives, per_device(): lax.all_gather(attended, 'tp', axis=1, tiled=True)  3.41 us
  transfers between devices with their start and end apart: 8, of which 2 were waited for; matrix products, arithmetic and copies ran while one was open for 17% of the time, Pallas kernels for 0%

commit v1 on v0

v1 whole, which is shorter than its diff:
```python
import functools

import jax
import jax.numpy as jnp
from jax import lax
from jax.experimental import pallas as pl
from jax.experimental.pallas import tpu as pltpu
from jax.sharding import PartitionSpec as P

HEAD_DIM = 128
SIDE_KEY_COUNT = 64
MIDDLE_DILATION = 4
FAR_DILATION = 16
NEG = -1e30
LOG2E = 1.4426950408889634
EXP_SCALE = HEAD_DIM ** (-0.5) * LOG2E


def iota(shape, dim):
    return lax.broadcasted_iota(jnp.int32, shape, dim)


def class_major(rows):
    per = rows // FAR_DILATION
    out_row, in_row = iota((rows, rows), 0), iota((rows, rows), 1)
    return jnp.where(in_row == FAR_DILATION * (out_row % per) + out_row // per, 1.0, 0.0)


def token_order(rows):
    per = rows // FAR_DILATION
    out_row, in_row = iota((rows, rows), 0), iota((rows, rows), 1)
    return jnp.where(out_row == FAR_DILATION * (in_row % per) + in_row // per, 1.0, 0.0)


def dot(a, b):
    return jnp.dot(a, b, preferred_element_type=jnp.float32)


def dot_t(a, b):
    return lax.dot_general(a, b, (((1,), (1,)), ((), ())), preferred_element_type=jnp.float32)


def spread_kernel(group, arrays, *refs):
    ins, outs = refs[:arrays], refs[arrays:]
    me = lax.rem(lax.axis_index("sp"), group)
    order = class_major(ins[0].shape[0]).astype(jnp.bfloat16)
    for k in range(group):
        head = me ^ k
        cols = pl.ds(pl.multiple_of(head * HEAD_DIM, HEAD_DIM), HEAD_DIM)
        part = jnp.concatenate([ref[:, cols] for ref in ins], axis=1)
        outs[k][...] = dot(order, part).astype(jnp.bfloat16)


def spread(group, *arrays):
    rows = arrays[0].shape[0]
    out = jax.ShapeDtypeStruct((rows, HEAD_DIM * len(arrays)), jnp.bfloat16)
    return pl.pallas_call(
        functools.partial(spread_kernel, group, len(arrays)),
        out_shape=[out] * group,
        in_specs=[pl.BlockSpec(memory_space=pltpu.VMEM)] * len(arrays),
        out_specs=[pl.BlockSpec(memory_space=pltpu.VMEM)] * group,
        cost_estimate=pl.CostEstimate(flops=10**6, bytes_accessed=10**6, transcendentals=0),
    )(*arrays)


def attend_kernel(group, groups, *refs):
    q_in, kv_in = refs[:group], refs[group : 4 * group]
    outs = refs[4 * group : 5 * group]
    q_s, kv_s, num_s, top_s, den_s, out_s, bias16, bias4, bias1, sems = refs[5 * group :]
    rows = q_s.shape[1]
    per = rows // FAR_DILATION
    quarter = FAR_DILATION // MIDDLE_DILATION
    mid_rows = per * quarter
    here = lax.axis_index("sp")
    me, mine = lax.rem(here, group), here // group
    even = lax.rem(mine, 2) == 0
    first, last = mine == 0, mine == groups - 1

    copies = []
    for k in range(group):
        member = me ^ k
        copies.append(pltpu.make_async_copy(q_in[k], q_s.at[member], sems.at[k]))
        bases = (group, jnp.where(even, 2 * group, 0), jnp.where(even, 0, 2 * group))
        for j, base in enumerate(bases):
            slot = kv_s.at[base + member]
            copies.append(
                pltpu.make_async_copy(kv_in[j * group + k], slot, sems.at[(j + 1) * group + k])
            )
    for copy in copies:
        copy.start()

    side = SIDE_KEY_COUNT
    far_q, far_k = group * per, 3 * group * per
    q_pos, k_pos = iota((far_q, far_k), 0), iota((far_q, far_k), 1) - group * per
    near = jnp.abs(k_pos - q_pos) <= side
    near &= (k_pos >= jnp.where(first, 0, -far_q)) & (k_pos < jnp.where(last, far_q, 2 * far_q))
    bias16[...] = jnp.where(near, 0.0, NEG)

    q_row, k_row = iota((mid_rows, 3 * mid_rows), 0), iota((mid_rows, 3 * mid_rows), 1)
    q_pos = quarter * (q_row % per) + q_row // per
    k_pos = quarter * (k_row % per) + (k_row // per) % quarter + (k_row // mid_rows - 1) * mid_rows
    near = jnp.abs(k_pos - q_pos) <= side
    for b in range(group):
        ok = near
        if b == 0:
            ok &= k_pos >= jnp.where(first, 0, -mid_rows)
        if b == group - 1:
            ok &= k_pos < jnp.where(last, mid_rows, 2 * mid_rows)
        bias4[b] = jnp.where(ok, 0.0, NEG)

    q_row, k_row = iota((rows, rows), 0), iota((rows, rows), 1)
    q_pos = FAR_DILATION * (q_row % per) + q_row // per
    k_pos = FAR_DILATION * (k_row % per) + k_row // per
    bias1[:, :rows] = jnp.where(jnp.abs(k_pos - q_pos) <= side, 0.0, NEG)
    q_row, k_row = iota((rows, 2 * side), 0), iota((rows, 2 * side), 1)
    q_pos = FAR_DILATION * (q_row % per) + q_row // per
    k_pos = jnp.where(k_row < side, k_row - side, rows + k_row - side)
    bias1[:, rows:] = jnp.where(jnp.abs(k_pos - q_pos) <= side, 0.0, NEG)

    def scores_of(q, keys, bias):
        return dot_t(q, keys) + bias

    def weigh(scores, values, top):
        raised = jnp.exp2((scores - top) * EXP_SCALE).astype(jnp.bfloat16)
        both = dot(raised, jnp.concatenate([values, jnp.ones_like(values)], axis=1))
        return both[:, :HEAD_DIM], both[:, HEAD_DIM:]

    for copy in copies:
        copy.wait()

    def far(c, _):
        at = pl.ds(pl.multiple_of(c * per, per), per)
        q = q_s[:, at, :].reshape(far_q, HEAD_DIM)
        keys = kv_s[:, at, :HEAD_DIM].reshape(far_k, HEAD_DIM)
        values = kv_s[:, at, HEAD_DIM:].reshape(far_k, HEAD_DIM)
        scores = scores_of(q, keys, bias16[...])
        top = jnp.max(scores, axis=1, keepdims=True)
        num, den = weigh(scores, values, top)
        num_s[:, at, :] = num.reshape(group, per, HEAD_DIM)
        den_s[:, at, :] = den.reshape(group, per, HEAD_DIM)
        top_s[:, at, :] = jnp.broadcast_to(top, num.shape).reshape(group, per, HEAD_DIM)
        return 0

    lax.fori_loop(0, FAR_DILATION, far, 0, unroll=4)

    def join(old, new):
        (num_a, den_a, top_a), (num_b, den_b, top_b) = old, new
        top = jnp.maximum(top_a, top_b)
        by_a, by_b = jnp.exp2((top_a - top) * EXP_SCALE), jnp.exp2((top_b - top) * EXP_SCALE)
        return num_a * by_a + num_b * by_b, den_a * by_a + den_b * by_b, top

    def middle(step, _):
        b = step // MIDDLE_DILATION
        residue = lax.rem(step, MIDDLE_DILATION)
        ats = [
            pl.ds(pl.multiple_of((MIDDLE_DILATION * s + residue) * per, per), per)
            for s in range(quarter)
        ]
        q = jnp.concatenate([q_s[b, at, :] for at in ats], axis=0)
        slots = [group - 1 + b + j for j in range(3)]
        keys = jnp.concatenate([kv_s[j, at, :HEAD_DIM] for j in slots for at in ats], axis=0)
        values = jnp.concatenate([kv_s[j, at, HEAD_DIM:] for j in slots for at in ats], axis=0)
        scores = scores_of(q, keys, bias4[b])
        top = jnp.max(scores, axis=1, keepdims=True)
        num, den = weigh(scores, values, top)
        old = [jnp.concatenate([ref[b, at, :] for at in ats], axis=0) for ref in (num_s, den_s, top_s)]
        new = join(old, (num, den, top))
        for ref, value in zip((num_s, den_s, top_s), new):
            for s, at in enumerate(ats):
                ref[b, at, :] = value[s * per : (s + 1) * per]
        return 0

    lax.fori_loop(0, group * MIDDLE_DILATION, middle, 0, unroll=4)

    token = iota((side, rows), 0)
    column = iota((side, rows), 1)
    column = FAR_DILATION * (column % per) + column // per
    ends = jnp.where(column == token, 1.0, 0.0).astype(jnp.bfloat16)
    tails = jnp.where(column == token + rows - side, 1.0, 0.0).astype(jnp.bfloat16)
    natural = token_order(rows).astype(jnp.bfloat16)
    half = rows // 2
    for b in range(group):
        own = kv_s[group + b]
        beside = jnp.concatenate([dot(tails, kv_s[group + b - 1]), dot(ends, kv_s[group + b + 1])], axis=0)
        beside = beside.astype(jnp.bfloat16)
        values = jnp.concatenate([own[:, HEAD_DIM:], beside[:, HEAD_DIM:]], axis=0)
        column = iota((1, 2 * side), 1)
        edge = jnp.zeros((1, 2 * side), jnp.float32)
        if b == 0:
            edge += jnp.where((column < side) & first, NEG, 0.0)
        if b == group - 1:
            edge += jnp.where((column >= side) & last, NEG, 0.0)
        for part in range(2):
            at = pl.ds(part * half, half)
            q = q_s[b, at, :]
            inner = scores_of(q, own[:, :HEAD_DIM], bias1[at, :rows])
            outer = scores_of(q, beside[:, :HEAD_DIM], bias1[at, rows:])
            if b in (0, group - 1):
                outer += edge
            scores = jnp.concatenate([inner, outer], axis=1)
            top = jnp.max(scores, axis=1, keepdims=True)
            num, den = weigh(scores, values, top)
            num, den, _ = join((num_s[b, at, :], den_s[b, at, :], top_s[b, at, :]), (num, den, top))
            out_s[b, at, :] = (num / den).astype(jnp.bfloat16)
    for k in range(group):
        outs[k][...] = dot(natural, out_s[me ^ k]).astype(jnp.bfloat16)


def attend(group, groups, q, own, even, odd):
    rows = q[0].shape[0]
    per = rows // FAR_DILATION
    mid_rows = per * (FAR_DILATION // MIDDLE_DILATION)
    f32, bf16 = jnp.float32, jnp.bfloat16
    return pl.pallas_call(
        functools.partial(attend_kernel, group, groups),
        out_shape=[jax.ShapeDtypeStruct((rows, HEAD_DIM), bf16)] * group,
        in_specs=[pl.BlockSpec(memory_space=pl.ANY)] * (4 * group),
        out_specs=[pl.BlockSpec(memory_space=pltpu.VMEM)] * group,
        scratch_shapes=[
            pltpu.VMEM((group, rows, HEAD_DIM), bf16),
            pltpu.VMEM((3 * group, rows, 2 * HEAD_DIM), bf16),
            pltpu.VMEM((group, rows, HEAD_DIM), f32),
            pltpu.VMEM((group, rows, HEAD_DIM), f32),
            pltpu.VMEM((group, rows, HEAD_DIM), f32),
            pltpu.VMEM((group, rows, HEAD_DIM), bf16),
            pltpu.VMEM((group * per, 3 * group * per), f32),
            pltpu.VMEM((group, mid_rows, 3 * mid_rows), f32),
            pltpu.VMEM((rows, rows + 2 * SIDE_KEY_COUNT), f32),
            pltpu.SemaphoreType.DMA((4 * group,)),
        ],
        cost_estimate=pl.CostEstimate(flops=10**9, bytes_accessed=10**6, transcendentals=10**6),
    )(*q, *own, *even, *odd)


def project_kernel(group, *refs):
    own, other = refs[:group], refs[group : 2 * group]
    w_ref, out_ref = refs[2 * group :]
    me, side = lax.rem(lax.axis_index("sp"), group), lax.axis_index("tp")
    total = None
    for k in range(group):
        left = jnp.concatenate([own[k][...], other[k][...]], axis=1)
        right = []
        for core in (side, 1 - side):
            row = (core * group + (me ^ k)) * HEAD_DIM
            right.append(w_ref[pl.ds(pl.multiple_of(row, HEAD_DIM), HEAD_DIM), :])
        term = dot(left, jnp.concatenate(right, axis=0))
        total = term if total is None else total + term
    out_ref[...] = total.astype(jnp.bfloat16)


def project(group, own, other, w_out):
    rows, width = own[0].shape[0], w_out.shape[1]
    tile = 256
    piece = pl.BlockSpec((rows, HEAD_DIM), lambda j: (0, 0))
    return pl.pallas_call(
        functools.partial(project_kernel, group),
        out_shape=jax.ShapeDtypeStruct((rows, width), jnp.bfloat16),
        grid=(width // tile,),
        in_specs=[piece] * (2 * group) + [pl.BlockSpec((w_out.shape[0], tile), lambda j: (0, j))],
        out_specs=pl.BlockSpec((rows, tile), lambda j: (0, j)),
        cost_estimate=pl.CostEstimate(flops=10**9, bytes_accessed=10**6, transcendentals=0),
    )(*own, *other, w_out)


def per_device(queries, keys, values, w_out):
    rows = queries.shape[0]
    shards = lax.axis_size("sp")
    group = -(-(SIDE_KEY_COUNT * FAR_DILATION) // rows)
    groups = shards // group

    def inside(value, k):
        return lax.ppermute(value, "sp", [(s, s ^ k) for s in range(shards)])

    def across(value, parity):
        pairs = []
        for s in range(shards):
            mine = s // group
            beside = mine + 1 if mine % 2 == parity else mine - 1
            for t in range(2):
                if 0 <= beside < groups:
                    pairs.append((2 * s + t, 2 * (s + (beside - mine) * group) + t))
                else:
                    pairs.append((2 * s + t, 2 * s + 1 - t))
        return lax.ppermute(value, ("sp", "tp"), pairs)

    def other_core(value):
        return lax.ppermute(value, "tp", [(0, 1), (1, 0)])

    kv = spread(group, keys, values)
    q = spread(group, queries)
    own = [kv[0]] + [inside(kv[k], k) for k in range(1, group)]
    even = [across(piece, 0) for piece in own]
    odd = [across(piece, 1) for piece in own]
    q = [q[0]] + [inside(q[k], k) for k in range(1, group)]
    out = attend(group, groups, q, own, even, odd)
    out = [out[0]] + [inside(out[k], k) for k in range(1, group)]
    return project(group, out, [other_core(piece) for piece in out], w_out)


def solution(mesh):
    in_specs = (P("sp", "tp"), P("sp", "tp"), P("sp", "tp"), P(None, "tp"))
    out_specs = P("sp", "tp")
    return jax.shard_map(
        per_device, mesh=mesh, in_specs=in_specs, out_specs=out_specs, check_vma=False
    )
```

time: 141 us -> 58.8 us (0.42)
  the two profiles are of different devices: /device:TPU:17 before, /device:TPU:0 now
where the time goes in v1:
time: 58.8 us; the launch traced here: 58.5 us
  Pallas kernels  21.8 us (37%)
  starting transfers between devices  19.4 us (33%)
  waiting for transfers between devices  15.9 us (27%)
  local copies, waits for them, and re-layouts  1.23 us (2%)
    pallas_call x1, Pallas kernels, attend(): pl.pallas_call(functools.partial(attend_kernel, group, groups), out_shape...  13.6 us
    ppermute x9, starting transfers between devices, inside(): return lax.ppermute(value, 'sp', [(s, s ^ k) for s in range(shards)])  12.5 us
    ppermute x9, waiting for transfers between devices, inside(): return lax.ppermute(value, 'sp', [(s, s ^ k) for s in range(shards)])  9.29 us
    ppermute x8, starting transfers between devices, across(): return lax.ppermute(value, ('sp', 'tp'), pairs)  6.92 us
    ppermute x8, waiting for transfers between devices, across(): return lax.ppermute(value, ('sp', 'tp'), pairs)  5.38 us
    pallas_call x1, Pallas kernels, project(): pl.pallas_call(functools.partial(project_kernel, group), out_shape=jax.Sh...  4.2 us
    pallas_call x2, Pallas kernels, spread(): pl.pallas_call(functools.partial(spread_kernel, group, len(arrays)), out_...  3.97 us
    unnamed x42, local copies, waits for them, and re-layouts  1.23 us
  transfers between devices with their start and end apart: 21, of which 8 were waited for; matrix products, arithmetic and copies ran while one was open for 0% of the time, Pallas kernels for 3%

profile of v1, /device:TPU:0, one launch (start us, length us, event | category | flops | bytes accessed | tf_op | source)
XLA Modules:
  0.0 58.5 jit_solution(1755272633977362542)
XLA Ops:
  0.0 2.1 %shard_map.47 = (bf16[256,256]{1,0:T(8,128)(2,1)}, bf16[256,256]{1,0:T(8,128)(2,1)}, bf16[256,256]{1,0:T(8,128)(2,1)}, bf16[256,256]{1,0:T(8,128)(2,1)}) custom-call(bf16[256,512]{1,0:T(8,128)(2,1)} %refs_0_.3, bf16[256,512]{1,0:T(8,128)(2,1)} %refs_1_.1), custom_call_target="tpu_custom_call" | custom-call | flops 1000000 | bytes 1000000 | tf_op jit(solution)/shard_map/pallas_call | solution.py:57
  2.1 3.0 %collective-permute-start.3 = (bf16[256,256]{1,0:T(8,128)(2,1)}, bf16[256,256]{1,0:T(8,128)(2,1)S(1)}, u32[]{:S(2)}, u32[]{:S(2)}) collective-permute-start(bf16[256,256]{1,0:T(8,128)(2,1)} %get-tuple-element.22), channel_id=1, source_target_pairs={{0,2},{2,0},{4,6},{6,4},{8,10},{10,8},{12,14},{14,12},{16,18},{18,... | collective-permute-start | bytes 393224 | tf_op jit(solution)/shard_map/ppermute | solution.py:272
  5.0 1.9 %shard_map.46 = (bf16[256,128]{1,0:T(8,128)(2,1)}, bf16[256,128]{1,0:T(8,128)(2,1)}, bf16[256,128]{1,0:T(8,128)(2,1)}, bf16[256,128]{1,0:T(8,128)(2,1)}) custom-call(bf16[256,512]{1,0:T(8,128)(2,1)} %refs_0_.2), custom_call_target="tpu_custom_call" | custom-call | flops 1000000 | bytes 1000000 | tf_op jit(solution)/shard_map/pallas_call | solution.py:57
  6.9 0.0 collective-permute-start
  7.0 2.1 %collective-permute-start.1 = (bf16[256,128]{1,0:T(8,128)(2,1)}, bf16[256,128]{1,0:T(8,128)(2,1)S(1)}, u32[]{:S(2)}, u32[]{:S(2)}) collective-permute-start(bf16[256,128]{1,0:T(8,128)(2,1)} %get-tuple-element.19), channel_id=1, source_target_pairs={{0,4},{2,6},{4,0},{6,2},{8,12},{10,14},{12,8},{14,10},{16,20},{18,... | collective-permute-start | bytes 196616 | tf_op jit(solution)/shard_map/ppermute | solution.py:272
  9.0 1.4 %collective-permute-start.2 = (bf16[256,128]{1,0:T(8,128)(2,1)}, bf16[256,128]{1,0:T(8,128)(2,1)S(1)}, u32[]{:S(2)}, u32[]{:S(2)}) collective-permute-start(bf16[256,128]{1,0:T(8,128)(2,1)} %get-tuple-element.20), channel_id=1, source_target_pairs={{0,6},{2,4},{4,2},{6,0},{8,14},{10,12},{12,10},{14,8},{16,22},{18,... | collective-permute-start | bytes 196616 | tf_op jit(solution)/shard_map/ppermute | solution.py:272
  10.4 1.5 %collective-permute-start.4 = (bf16[256,256]{1,0:T(8,128)(2,1)}, bf16[256,256]{1,0:T(8,128)(2,1)S(1)}, u32[]{:S(2)}, u32[]{:S(2)}) collective-permute-start(bf16[256,256]{1,0:T(8,128)(2,1)} %get-tuple-element.23), channel_id=1, source_target_pairs={{0,4},{2,6},{4,0},{6,2},{8,12},{10,14},{12,8},{14,10},{16,20},{18,... | collective-permute-start | bytes 393224 | tf_op jit(solution)/shard_map/ppermute | solution.py:272
  12.0 0.0 collective-permute-done.refs_1_
  12.0 1.0 %collective-permute-start.5 = (bf16[256,256]{1,0:T(8,128)(2,1)}, bf16[256,256]{1,0:T(8,128)(2,1)S(1)}, u32[]{:S(2)}, u32[]{:S(2)}) collective-permute-start(bf16[256,256]{1,0:T(8,128)(2,1)} %get-tuple-element.24), channel_id=1, source_target_pairs={{0,6},{2,4},{4,2},{6,0},{8,14},{10,12},{12,10},{14,8},{16,22},{18,... | collective-permute-start | bytes 393224 | tf_op jit(solution)/shard_map/ppermute | solution.py:272
  12.9 0.0 collective-permute-done.1.refs_2_
  12.9 0.0 collective-permute-start.10
  12.9 1.8 %collective-permute-done.2.refs_3_ = bf16[256,128]{1,0:T(8,128)(2,1)S(1)} collective-permute-done((bf16[256,128]{1,0:T(8,128)(2,1)}, bf16[256,128]{1,0:T(8,128)(2,1)S(1)}, u32[]{:S(2)}, u32[]{:S(2)}) %collective-permute-start.2) | collective-permute-done | bytes 65568 | tf_op jit(solution)/shard_map/ppermute | solution.py:272
  14.8 1.6 %collective-permute-start.6 = (bf16[256,256]{1,0:T(8,128)(2,1)}, bf16[256,256]{1,0:T(8,128)(2,1)S(1)}, u32[]{:S(2)}, u32[]{:S(2)}) collective-permute-start(bf16[256,256]{1,0:T(8,128)(2,1)} %get-tuple-element.21.refs_4_), channel_id=1, source_target_pairs={{0,8},{1,9},{2,10},{3,11},{4,12},{5,13},{6,14},{7,15},{8,0},{9,1},... | collective-permute-start | bytes 393224 | tf_op jit(solution)/shard_map/ppermute | solution.py:284
  16.3 0.0 collective-permute-done.3.refs_5_
  16.3 0.0 collective-permute-start.11
  16.3 2.5 %collective-permute-done.4.refs_6_ = bf16[256,256]{1,0:T(8,128)(2,1)S(1)} collective-permute-done((bf16[256,256]{1,0:T(8,128)(2,1)}, bf16[256,256]{1,0:T(8,128)(2,1)S(1)}, u32[]{:S(2)}, u32[]{:S(2)}) %collective-permute-start.4) | collective-permute-done | bytes 131104 | tf_op jit(solution)/shard_map/ppermute | solution.py:272
  18.9 1.7 %collective-permute-start.7 = (bf16[256,256]{1,0:T(8,128)(2,1)S(1)}, bf16[256,256]{1,0:T(8,128)(2,1)S(1)}, u32[]{:S(2)}, u32[]{:S(2)}) collective-permute-start(bf16[256,256]{1,0:T(8,128)(2,1)S(1)} %collective-permute-done.3.refs_5_), channel_id=1, source_target_pairs={{0,8},{1,9},{2,10},{3,11},{4,12},{5,13},{6,14},{7,15},{8,0},{9,1},... | collective-permute-start | bytes 393224 | tf_op jit(solution)/shard_map/ppermute | solution.py:284
  20.6 0.0 collective-permute-done.5.refs_7_
  20.6 0.0 collective-permute-start.12
  20.6 0.0 collective-permute-done.10.refs_12_
  20.6 0.0 copy-start.3
  20.6 3.1 %collective-permute-start.8 = (bf16[256,256]{1,0:T(8,128)(2,1)S(1)}, bf16[256,256]{1,0:T(8,128)(2,1)S(1)}, u32[]{:S(2)}, u32[]{:S(2)}) collective-permute-start(bf16[256,256]{1,0:T(8,128)(2,1)S(1)} %collective-permute-done.4.refs_6_), channel_id=1, source_target_pairs={{0,8},{1,9},{2,10},{3,11},{4,12},{5,13},{6,14},{7,15},{8,0},{9,1},... | collective-permute-start | bytes 393224 | tf_op jit(solution)/shard_map/ppermute | solution.py:284
  23.7 0.0 collective-permute-done.6.refs_8_
  23.7 0.0 collective-permute-start.13
  23.7 0.0 collective-permute-done.11.refs_13_
  23.7 0.0 copy-start.5
  23.8 0.5 collective-permute-start.9
  24.3 0.0 collective-permute-done.7.refs_9_
  24.3 0.0 collective-permute-done.12.refs_14_
  24.3 3.2 %collective-permute-done.8.refs_10_ = bf16[256,256]{1,0:T(8,128)(2,1)S(1)} collective-permute-done((bf16[256,256]{1,0:T(8,128)(2,1)S(1)}, bf16[256,256]{1,0:T(8,128)(2,1)S(1)}, u32[]{:S(2)}, u32[]{:S(2)}) %collective-permute-start.8) | collective-permute-done | bytes 131104 | tf_op jit(solution)/shard_map/ppermute | solution.py:284
  27.4 0.0 collective-permute-done.13.refs_15_
  27.5 2.2 %collective-permute-done.9.refs_11_ = bf16[256,256]{1,0:T(8,128)(2,1)S(1)} collective-permute-done((bf16[256,256]{1,0:T(8,128)(2,1)S(1)}, bf16[256,256]{1,0:T(8,128)(2,1)S(1)}, u32[]{:S(2)}, u32[]{:S(2)}) %collective-permute-start.9) | collective-permute-done | bytes 131104 | tf_op jit(solution)/shard_map/ppermute | solution.py:284
  29.6 0.0 copy-done.11
  29.6 0.0 copy-done.12
  29.7 0.0 copy-done.13
  29.7 0.0 copy-done
  29.7 0.0 copy-done.1
  29.7 0.0 copy-done.2
  29.7 0.0 copy-done.3
  29.7 0.0 copy-done.4
  29.7 0.0 copy-done.5
  29.7 0.0 copy-done.6
  29.7 0.0 copy-done.7
  29.7 0.0 copy-done.8
  29.8 0.5 copy-done.10
  30.3 13.6 %shard_map.48 = (bf16[256,128]{1,0:T(8,128)(2,1)}, bf16[256,128]{1,0:T(8,128)(2,1)}, bf16[256,128]{1,0:T(8,128)(2,1)}, bf16[256,128]{1,0:T(8,128)(2,1)}) custom-call(bf16[256,128]{1,0:T(8,128)(2,1)} %get-tuple-element.17.refs_0_, bf16[256,128]{1,0:T(8,128)(2,1)} %copy-done.11, bf16[256,128]{1,0:T(8,128)(2,1)} %copy-done.12, bf16[256,128]{1,0:T(8,128)(2,1)} %copy-done.13, ...), custom_call_target="tpu_custom_call" | custom-call | flops 1000000000 | bytes 1000000 | tf_op jit(solution)/shard_map/pallas_call | solution.py:214
  43.9 1.3 %collective-permute-start.14 = (bf16[256,128]{1,0:T(8,128)(2,1)}, bf16[256,128]{1,0:T(8,128)(2,1)S(1)}, u32[]{:S(2)}, u32[]{:S(2)}) collective-permute-start(bf16[256,128]{1,0:T(8,128)(2,1)} %get-tuple-element.26), channel_id=1, source_target_pairs={{0,2},{2,0},{4,6},{6,4},{8,10},{10,8},{12,14},{14,12},{16,18},{18,... | collective-permute-start | bytes 196616 | tf_op jit(solution)/shard_map/ppermute | solution.py:272
  45.2 1.8 %collective-permute-start.15 = (bf16[256,128]{1,0:T(8,128)(2,1)}, bf16[256,128]{1,0:T(8,128)(2,1)S(1)}, u32[]{:S(2)}, u32[]{:S(2)}) collective-permute-start(bf16[256,128]{1,0:T(8,128)(2,1)} %get-tuple-element.27), channel_id=1, source_target_pairs={{0,4},{2,6},{4,0},{6,2},{8,12},{10,14},{12,8},{14,10},{16,20},{18,... | collective-permute-start | bytes 196616 | tf_op jit(solution)/shard_map/ppermute | solution.py:272
  47.0 0.4 collective-permute-start.16
  47.4 0.0 collective-permute-start.17
  47.4 1.0 %collective-permute-done.14.refs_1_ = bf16[256,128]{1,0:T(8,128)(2,1)S(1)} collective-permute-done((bf16[256,128]{1,0:T(8,128)(2,1)}, bf16[256,128]{1,0:T(8,128)(2,1)S(1)}, u32[]{:S(2)}, u32[]{:S(2)}) %collective-permute-start.14) | collective-permute-done | bytes 65568 | tf_op jit(solution)/shard_map/ppermute | solution.py:272
  48.4 0.0 collective-permute-start.18
  48.4 1.2 %collective-permute-done.15.refs_2_ = bf16[256,128]{1,0:T(8,128)(2,1)S(1)} collective-permute-done((bf16[256,128]{1,0:T(8,128)(2,1)}, bf16[256,128]{1,0:T(8,128)(2,1)S(1)}, u32[]{:S(2)}, u32[]{:S(2)}) %collective-permute-start.15) | collective-permute-done | bytes 65568 | tf_op jit(solution)/shard_map/ppermute | solution.py:272
  49.6 0.0 collective-permute-start.19
  49.6 2.7 %collective-permute-done.16.refs_3_ = bf16[256,128]{1,0:T(8,128)(2,1)S(1)} collective-permute-done((bf16[256,128]{1,0:T(8,128)(2,1)}, bf16[256,128]{1,0:T(8,128)(2,1)S(1)}, u32[]{:S(2)}, u32[]{:S(2)}) %collective-permute-start.16) | collective-permute-done | bytes 65568 | tf_op jit(solution)/shard_map/ppermute | solution.py:272
  52.4 0.0 collective-permute-start.20
  52.4 0.0 collective-permute-done.17.refs_4_
  52.4 0.0 collective-permute-done.18.refs_5_
  52.4 0.0 collective-permute-done.19.refs_6_
  52.4 0.0 copy-start.19
  52.4 1.2 %collective-permute-done.20.refs_7_ = bf16[256,128]{1,0:T(8,128)(2,1)S(1)} collective-permute-done((bf16[256,128]{1,0:T(8,128)(2,1)S(1)}, bf16[256,128]{1,0:T(8,128)(2,1)S(1)}, u32[]{:S(2)}, u32[]{:S(2)}) %collective-permute-start.20) | collective-permute-done | bytes 65568 | tf_op jit(solution)/shard_map/ppermute | solution.py:287
  53.6 0.0 copy-done.14
  53.7 0.6 %copy-done.20 = bf16[256,128]{1,0:T(8,128)(2,1)} copy-done((bf16[256,128]{1,0:T(8,128)(2,1)}, bf16[256,128]{1,0:T(8,128)(2,1)S(1)}, u32[]{:S(2)}) %copy-start.20) | copy-done | bytes 65560
  54.3 4.2 %shard_map.49 = bf16[256,1024]{1,0:T(8,128)(2,1)} custom-call(bf16[256,128]{1,0:T(8,128)(2,1)} %get-tuple-element.25.refs_0_, bf16[256,128]{1,0:T(8,128)(2,1)} %copy-done.14, bf16[256,128]{1,0:T(8,128)(2,1)} %copy-done.15, bf16[256,128]{1,0:T(8,128)(2,1)} %copy-done.16, bf16[256,128]{1,0:T(8,128)(2,1)} %copy-done.17, bf16[256,128]{1,0:T(8,128)(2,1)} %copy-done.18, ...), custom_call_target="tpu_custom_call" | custom-call | flops 1000000000 | bytes 1000000 | tf_op jit(solution)/shard_map/pallas_call | solution.py:255
  (24 shorter events, 0.0 us)
Async XLA Ops:
  2.1 14.3 %collective-permute-start.3 = (bf16[256,256]{1,0:T(8,128)(2,1)}, bf16[256,256]{1,0:T(8,128)(2,1)S(1)}, u32[]{:S(2)}, u32[]{:S(2)}) collective-permute-start(bf16[256,256]{1,0:T(8,128)(2,1)} %get-tuple-element.22), channel_id=1, source_target_pairs={{0,2},{2,0},{4,6},{6,4},{8,10},{10,8},{12,14},{14,12},{16,18},{18,... | collective-permute-start | bytes 393224 | tf_op jit(solution)/shard_map/ppermute | solution.py:272
  6.9 5.0 %collective-permute-start = (bf16[256,128]{1,0:T(8,128)(2,1)}, bf16[256,128]{1,0:T(8,128)(2,1)S(1)}, u32[]{:S(2)}, u32[]{:S(2)}) collective-permute-start(bf16[256,128]{1,0:T(8,128)(2,1)} %get-tuple-element.18), channel_id=1, source_target_pairs={{0,2},{2,0},{4,6},{6,4},{8,10},{10,8},{12,14},{14,12},{16,18},{18,... | collective-permute-start | bytes 196616 | tf_op jit(solution)/shard_map/ppermute | solution.py:272
  7.0 6.0 %collective-permute-start.1 = (bf16[256,128]{1,0:T(8,128)(2,1)}, bf16[256,128]{1,0:T(8,128)(2,1)S(1)}, u32[]{:S(2)}, u32[]{:S(2)}) collective-permute-start(bf16[256,128]{1,0:T(8,128)(2,1)} %get-tuple-element.19), channel_id=1, source_target_pairs={{0,4},{2,6},{4,0},{6,2},{8,12},{10,14},{12,8},{14,10},{16,20},{18,... | collective-permute-start | bytes 196616 | tf_op jit(solution)/shard_map/ppermute | solution.py:272
  9.0 5.8 %collective-permute-start.2 = (bf16[256,128]{1,0:T(8,128)(2,1)}, bf16[256,128]{1,0:T(8,128)(2,1)S(1)}, u32[]{:S(2)}, u32[]{:S(2)}) collective-permute-start(bf16[256,128]{1,0:T(8,128)(2,1)} %get-tuple-element.20), channel_id=1, source_target_pairs={{0,6},{2,4},{4,2},{6,0},{8,14},{10,12},{12,10},{14,8},{16,22},{18,... | collective-permute-start | bytes 196616 | tf_op jit(solution)/shard_map/ppermute | solution.py:272
  10.4 8.4 %collective-permute-start.4 = (bf16[256,256]{1,0:T(8,128)(2,1)}, bf16[256,256]{1,0:T(8,128)(2,1)S(1)}, u32[]{:S(2)}, u32[]{:S(2)}) collective-permute-start(bf16[256,256]{1,0:T(8,128)(2,1)} %get-tuple-element.23), channel_id=1, source_target_pairs={{0,4},{2,6},{4,0},{6,2},{8,12},{10,14},{12,8},{14,10},{16,20},{18,... | collective-permute-start | bytes 393224 | tf_op jit(solution)/shard_map/ppermute | solution.py:272
  12.0 17.7 %copy-start.11 = (bf16[256,128]{1,0:T(8,128)(2,1)}, bf16[256,128]{1,0:T(8,128)(2,1)S(1)}, u32[]{:S(2)}) copy-start(bf16[256,128]{1,0:T(8,128)(2,1)S(1)} %collective-permute-done.refs_1_) | copy-start | bytes 196612
  12.0 8.6 %collective-permute-start.5 = (bf16[256,256]{1,0:T(8,128)(2,1)}, bf16[256,256]{1,0:T(8,128)(2,1)S(1)}, u32[]{:S(2)}, u32[]{:S(2)}) collective-permute-start(bf16[256,256]{1,0:T(8,128)(2,1)} %get-tuple-element.24), channel_id=1, source_target_pairs={{0,6},{2,4},{4,2},{6,0},{8,14},{10,12},{12,10},{14,8},{16,22},{18,... | collective-permute-start | bytes 393224 | tf_op jit(solution)/shard_map/ppermute | solution.py:272
  12.9 16.7 %copy-start.12 = (bf16[256,128]{1,0:T(8,128)(2,1)}, bf16[256,128]{1,0:T(8,128)(2,1)S(1)}, u32[]{:S(2)}) copy-start(bf16[256,128]{1,0:T(8,128)(2,1)S(1)} %collective-permute-done.1.refs_2_) | copy-start | bytes 196612
  12.9 7.6 %collective-permute-start.10 = (bf16[256,256]{1,0:T(8,128)(2,1)}, bf16[256,256]{1,0:T(8,128)(2,1)S(1)}, u32[]{:S(2)}, u32[]{:S(2)}) collective-permute-start(bf16[256,256]{1,0:T(8,128)(2,1)} %get-tuple-element.21.refs_4_), channel_id=1, source_target_pairs={{0,1},{1,0},{2,3},{3,2},{4,5},{5,4},{6,7},{7,6},{8,16},{9,17},{10,... | collective-permute-start | bytes 393224 | tf_op jit(solution)/shard_map/ppermute | solution.py:284
  14.8 14.9 %copy-start.13 = (bf16[256,128]{1,0:T(8,128)(2,1)}, bf16[256,128]{1,0:T(8,128)(2,1)S(1)}, u32[]{:S(2)}) copy-start(bf16[256,128]{1,0:T(8,128)(2,1)S(1)} %collective-permute-done.2.refs_3_) | copy-start | bytes 196612
  14.8 9.0 %collective-permute-start.6 = (bf16[256,256]{1,0:T(8,128)(2,1)}, bf16[256,256]{1,0:T(8,128)(2,1)S(1)}, u32[]{:S(2)}, u32[]{:S(2)}) collective-permute-start(bf16[256,256]{1,0:T(8,128)(2,1)} %get-tuple-element.21.refs_4_), channel_id=1, source_target_pairs={{0,8},{1,9},{2,10},{3,11},{4,12},{5,13},{6,14},{7,15},{8,0},{9,1},... | collective-permute-start | bytes 393224 | tf_op jit(solution)/shard_map/ppermute | solution.py:284
  16.3 13.3 %copy-start = (bf16[256,256]{1,0:T(8,128)(2,1)}, bf16[256,256]{1,0:T(8,128)(2,1)S(1)}, u32[]{:S(2)}) copy-start(bf16[256,256]{1,0:T(8,128)(2,1)S(1)} %collective-permute-done.3.refs_5_) | copy-start | bytes 393220
  16.3 7.4 %collective-permute-start.11 = (bf16[256,256]{1,0:T(8,128)(2,1)S(1)}, bf16[256,256]{1,0:T(8,128)(2,1)S(1)}, u32[]{:S(2)}, u32[]{:S(2)}) collective-permute-start(bf16[256,256]{1,0:T(8,128)(2,1)S(1)} %collective-permute-done.3.refs_5_), channel_id=1, source_target_pairs={{0,1},{1,0},{2,3},{3,2},{4,5},{5,4},{6,7},{7,6},{8,16},{9,17},{10,... | collective-permute-start | bytes 393224 | tf_op jit(solution)/shard_map/ppermute | solution.py:284
  18.8 10.8 %copy-start.1 = (bf16[256,256]{1,0:T(8,128)(2,1)}, bf16[256,256]{1,0:T(8,128)(2,1)S(1)}, u32[]{:S(2)}) copy-start(bf16[256,256]{1,0:T(8,128)(2,1)S(1)} %collective-permute-done.4.refs_6_) | copy-start | bytes 393220
  18.9 5.4 %collective-permute-start.7 = (bf16[256,256]{1,0:T(8,128)(2,1)S(1)}, bf16[256,256]{1,0:T(8,128)(2,1)S(1)}, u32[]{:S(2)}, u32[]{:S(2)}) collective-permute-start(bf16[256,256]{1,0:T(8,128)(2,1)S(1)} %collective-permute-done.3.refs_5_), channel_id=1, source_target_pairs={{0,8},{1,9},{2,10},{3,11},{4,12},{5,13},{6,14},{7,15},{8,0},{9,1},... | collective-permute-start | bytes 393224 | tf_op jit(solution)/shard_map/ppermute | solution.py:284
  20.6 9.1 %copy-start.2 = (bf16[256,256]{1,0:T(8,128)(2,1)}, bf16[256,256]{1,0:T(8,128)(2,1)S(1)}, u32[]{:S(2)}) copy-start(bf16[256,256]{1,0:T(8,128)(2,1)S(1)} %collective-permute-done.5.refs_7_) | copy-start | bytes 393220
  20.6 3.7 %collective-permute-start.12 = (bf16[256,256]{1,0:T(8,128)(2,1)S(1)}, bf16[256,256]{1,0:T(8,128)(2,1)S(1)}, u32[]{:S(2)}, u32[]{:S(2)}) collective-permute-start(bf16[256,256]{1,0:T(8,128)(2,1)S(1)} %collective-permute-done.4.refs_6_), channel_id=1, source_target_pairs={{0,1},{1,0},{2,3},{3,2},{4,5},{5,4},{6,7},{7,6},{8,16},{9,17},{10,... | collective-permute-start | bytes 393224 | tf_op jit(solution)/shard_map/ppermute | solution.py:284
  20.6 9.1 %copy-start.3 = (bf16[256,256]{1,0:T(8,128)(2,1)}, bf16[256,256]{1,0:T(8,128)(2,1)S(1)}, u32[]{:S(2)}) copy-start(bf16[256,256]{1,0:T(8,128)(2,1)S(1)} %collective-permute-done.10.refs_12_) | copy-start | bytes 393220
  20.6 6.9 %collective-permute-start.8 = (bf16[256,256]{1,0:T(8,128)(2,1)S(1)}, bf16[256,256]{1,0:T(8,128)(2,1)S(1)}, u32[]{:S(2)}, u32[]{:S(2)}) collective-permute-start(bf16[256,256]{1,0:T(8,128)(2,1)S(1)} %collective-permute-done.4.refs_6_), channel_id=1, source_target_pairs={{0,8},{1,9},{2,10},{3,11},{4,12},{5,13},{6,14},{7,15},{8,0},{9,1},... | collective-permute-start | bytes 393224 | tf_op jit(solution)/shard_map/ppermute | solution.py:284
  23.7 6.0 %copy-start.4 = (bf16[256,256]{1,0:T(8,128)(2,1)}, bf16[256,256]{1,0:T(8,128)(2,1)S(1)}, u32[]{:S(2)}) copy-start(bf16[256,256]{1,0:T(8,128)(2,1)S(1)} %collective-permute-done.6.refs_8_) | copy-start | bytes 393220
  23.7 3.7 %collective-permute-start.13 = (bf16[256,256]{1,0:T(8,128)(2,1)S(1)}, bf16[256,256]{1,0:T(8,128)(2,1)S(1)}, u32[]{:S(2)}, u32[]{:S(2)}) collective-permute-start(bf16[256,256]{1,0:T(8,128)(2,1)S(1)} %collective-permute-done.5.refs_7_), channel_id=1, source_target_pairs={{0,1},{1,0},{2,3},{3,2},{4,5},{5,4},{6,7},{7,6},{8,16},{9,17},{10,... | collective-permute-start | bytes 393224 | tf_op jit(solution)/shard_map/ppermute | solution.py:284
  23.7 6.0 %copy-start.5 = (bf16[256,256]{1,0:T(8,128)(2,1)}, bf16[256,256]{1,0:T(8,128)(2,1)S(1)}, u32[]{:S(2)}) copy-start(bf16[256,256]{1,0:T(8,128)(2,1)S(1)} %collective-permute-done.11.refs_13_) | copy-start | bytes 393220
  23.8 5.9 %collective-permute-start.9 = (bf16[256,256]{1,0:T(8,128)(2,1)S(1)}, bf16[256,256]{1,0:T(8,128)(2,1)S(1)}, u32[]{:S(2)}, u32[]{:S(2)}) collective-permute-start(bf16[256,256]{1,0:T(8,128)(2,1)S(1)} %collective-permute-done.5.refs_7_), channel_id=1, source_target_pairs={{0,8},{1,9},{2,10},{3,11},{4,12},{5,13},{6,14},{7,15},{8,0},{9,1},... | collective-permute-start | bytes 393224 | tf_op jit(solution)/shard_map/ppermute | solution.py:284
  24.3 5.4 %copy-start.6 = (bf16[256,256]{1,0:T(8,128)(2,1)}, bf16[256,256]{1,0:T(8,128)(2,1)S(1)}, u32[]{:S(2)}) copy-start(bf16[256,256]{1,0:T(8,128)(2,1)S(1)} %collective-permute-done.7.refs_9_) | copy-start | bytes 393220
  24.3 5.4 %copy-start.7 = (bf16[256,256]{1,0:T(8,128)(2,1)}, bf16[256,256]{1,0:T(8,128)(2,1)S(1)}, u32[]{:S(2)}) copy-start(bf16[256,256]{1,0:T(8,128)(2,1)S(1)} %collective-permute-done.12.refs_14_) | copy-start | bytes 393220
  27.4 2.3 %copy-start.8 = (bf16[256,256]{1,0:T(8,128)(2,1)}, bf16[256,256]{1,0:T(8,128)(2,1)S(1)}, u32[]{:S(2)}) copy-start(bf16[256,256]{1,0:T(8,128)(2,1)S(1)} %collective-permute-done.8.refs_10_) | copy-start | bytes 393220
  27.5 2.3 %copy-start.9 = (bf16[256,256]{1,0:T(8,128)(2,1)}, bf16[256,256]{1,0:T(8,128)(2,1)S(1)}, u32[]{:S(2)}) copy-start(bf16[256,256]{1,0:T(8,128)(2,1)S(1)} %collective-permute-done.13.refs_15_) | copy-start | bytes 393220
  29.6 0.6 %copy-start.10 = (bf16[256,256]{1,0:T(8,128)(2,1)}, bf16[256,256]{1,0:T(8,128)(2,1)S(1)}, u32[]{:S(2)}) copy-start(bf16[256,256]{1,0:T(8,128)(2,1)S(1)} %collective-permute-done.9.refs_11_) | copy-start | bytes 393220
  43.9 4.5 %collective-permute-start.14 = (bf16[256,128]{1,0:T(8,128)(2,1)}, bf16[256,128]{1,0:T(8,128)(2,1)S(1)}, u32[]{:S(2)}, u32[]{:S(2)}) collective-permute-start(bf16[256,128]{1,0:T(8,128)(2,1)} %get-tuple-element.26), channel_id=1, source_target_pairs={{0,2},{2,0},{4,6},{6,4},{8,10},{10,8},{12,14},{14,12},{16,18},{18,... | collective-permute-start | bytes 196616 | tf_op jit(solution)/shard_map/ppermute | solution.py:272
  45.2 4.5 %collective-permute-start.15 = (bf16[256,128]{1,0:T(8,128)(2,1)}, bf16[256,128]{1,0:T(8,128)(2,1)S(1)}, u32[]{:S(2)}, u32[]{:S(2)}) collective-permute-start(bf16[256,128]{1,0:T(8,128)(2,1)} %get-tuple-element.27), channel_id=1, source_target_pairs={{0,4},{2,6},{4,0},{6,2},{8,12},{10,14},{12,8},{14,10},{16,20},{18,... | collective-permute-start | bytes 196616 | tf_op jit(solution)/shard_map/ppermute | solution.py:272
  47.0 5.4 %collective-permute-start.16 = (bf16[256,128]{1,0:T(8,128)(2,1)}, bf16[256,128]{1,0:T(8,128)(2,1)S(1)}, u32[]{:S(2)}, u32[]{:S(2)}) collective-permute-start(bf16[256,128]{1,0:T(8,128)(2,1)} %get-tuple-element.28), channel_id=1, source_target_pairs={{0,6},{2,4},{4,2},{6,0},{8,14},{10,12},{12,10},{14,8},{16,22},{18,... | collective-permute-start | bytes 196616 | tf_op jit(solution)/shard_map/ppermute | solution.py:272
  47.4 5.0 %collective-permute-start.17 = (bf16[256,128]{1,0:T(8,128)(2,1)}, bf16[256,128]{1,0:T(8,128)(2,1)S(1)}, u32[]{:S(2)}, u32[]{:S(2)}) collective-permute-start(bf16[256,128]{1,0:T(8,128)(2,1)} %get-tuple-element.25.refs_0_), channel_id=1, source_target_pairs={{0,1},{1,0},{2,3},{3,2},{4,5},{5,4},{6,7},{7,6},{8,9},{9,8},{10,11... | collective-permute-start | bytes 196616 | tf_op jit(solution)/shard_map/ppermute | solution.py:287
  48.4 5.2 %copy-start.14 = (bf16[256,128]{1,0:T(8,128)(2,1)}, bf16[256,128]{1,0:T(8,128)(2,1)S(1)}, u32[]{:S(2)}) copy-start(bf16[256,128]{1,0:T(8,128)(2,1)S(1)} %collective-permute-done.14.refs_1_) | copy-start | bytes 196612
  48.4 4.0 %collective-permute-start.18 = (bf16[256,128]{1,0:T(8,128)(2,1)S(1)}, bf16[256,128]{1,0:T(8,128)(2,1)S(1)}, u32[]{:S(2)}, u32[]{:S(2)}) collective-permute-start(bf16[256,128]{1,0:T(8,128)(2,1)S(1)} %collective-permute-done.14.refs_1_), channel_id=1, source_target_pairs={{0,1},{1,0},{2,3},{3,2},{4,5},{5,4},{6,7},{7,6},{8,9},{9,8},{10,11... | collective-permute-start | bytes 196616 | tf_op jit(solution)/shard_map/ppermute | solution.py:287
  49.6 4.0 %copy-start.15 = (bf16[256,128]{1,0:T(8,128)(2,1)}, bf16[256,128]{1,0:T(8,128)(2,1)S(1)}, u32[]{:S(2)}) copy-start(bf16[256,128]{1,0:T(8,128)(2,1)S(1)} %collective-permute-done.15.refs_2_) | copy-start | bytes 196612
  49.6 2.8 %collective-permute-start.19 = (bf16[256,128]{1,0:T(8,128)(2,1)S(1)}, bf16[256,128]{1,0:T(8,128)(2,1)S(1)}, u32[]{:S(2)}, u32[]{:S(2)}) collective-permute-start(bf16[256,128]{1,0:T(8,128)(2,1)S(1)} %collective-permute-done.15.refs_2_), channel_id=1, source_target_pairs={{0,1},{1,0},{2,3},{3,2},{4,5},{5,4},{6,7},{7,6},{8,9},{9,8},{10,11... | collective-permute-start | bytes 196616 | tf_op jit(solution)/shard_map/ppermute | solution.py:287
  52.4 1.3 %copy-start.16 = (bf16[256,128]{1,0:T(8,128)(2,1)}, bf16[256,128]{1,0:T(8,128)(2,1)S(1)}, u32[]{:S(2)}) copy-start(bf16[256,128]{1,0:T(8,128)(2,1)S(1)} %collective-permute-done.16.refs_3_) | copy-start | bytes 196612
  52.4 1.3 %collective-permute-start.20 = (bf16[256,128]{1,0:T(8,128)(2,1)S(1)}, bf16[256,128]{1,0:T(8,128)(2,1)S(1)}, u32[]{:S(2)}, u32[]{:S(2)}) collective-permute-start(bf16[256,128]{1,0:T(8,128)(2,1)S(1)} %collective-permute-done.16.refs_3_), channel_id=1, source_target_pairs={{0,1},{1,0},{2,3},{3,2},{4,5},{5,4},{6,7},{7,6},{8,9},{9,8},{10,11... | collective-permute-start | bytes 196616 | tf_op jit(solution)/shard_map/ppermute | solution.py:287
  52.4 1.3 %copy-start.17 = (bf16[256,128]{1,0:T(8,128)(2,1)}, bf16[256,128]{1,0:T(8,128)(2,1)S(1)}, u32[]{:S(2)}) copy-start(bf16[256,128]{1,0:T(8,128)(2,1)S(1)} %collective-permute-done.17.refs_4_) | copy-start | bytes 196612
  52.4 1.2 %copy-start.18 = (bf16[256,128]{1,0:T(8,128)(2,1)}, bf16[256,128]{1,0:T(8,128)(2,1)S(1)}, u32[]{:S(2)}) copy-start(bf16[256,128]{1,0:T(8,128)(2,1)S(1)} %collective-permute-done.18.refs_5_) | copy-start | bytes 196612
  52.4 1.2 %copy-start.19 = (bf16[256,128]{1,0:T(8,128)(2,1)}, bf16[256,128]{1,0:T(8,128)(2,1)S(1)}, u32[]{:S(2)}) copy-start(bf16[256,128]{1,0:T(8,128)(2,1)S(1)} %collective-permute-done.19.refs_6_) | copy-start | bytes 196612
  53.7 0.6 %copy-start.20 = (bf16[256,128]{1,0:T(8,128)(2,1)}, bf16[256,128]{1,0:T(8,128)(2,1)S(1)}, u32[]{:S(2)}) copy-start(bf16[256,128]{1,0:T(8,128)(2,1)S(1)} %collective-permute-done.20.refs_7_) | copy-start | bytes 196612

commit v2 on v1

v2 whole, which is shorter than its diff:
```python
import functools

import jax
import jax.numpy as jnp
from jax import lax
from jax.experimental import pallas as pl
from jax.experimental.pallas import tpu as pltpu
from jax.sharding import PartitionSpec as P

HEAD_DIM = 128
SIDE_KEY_COUNT = 64
MIDDLE_DILATION = 4
FAR_DILATION = 16
NEG = -1e30
VMEM_LIMIT = 16 * 2**20
LOCAL_FLOPS = 10**9
LOG2E = 1.4426950408889634
EXP_SCALE = HEAD_DIM ** (-0.5) * LOG2E


def iota(shape, dim):
    return lax.broadcasted_iota(jnp.int32, shape, dim)


def class_major(rows):
    per = rows // FAR_DILATION
    out_row, in_row = iota((rows, rows), 0), iota((rows, rows), 1)
    return jnp.where(in_row == FAR_DILATION * (out_row % per) + out_row // per, 1.0, 0.0)


def token_order(rows):
    per = rows // FAR_DILATION
    out_row, in_row = iota((rows, rows), 0), iota((rows, rows), 1)
    return jnp.where(out_row == FAR_DILATION * (in_row % per) + in_row // per, 1.0, 0.0)


def dot(a, b):
    return jnp.dot(a, b, preferred_element_type=jnp.float32)


def dot_t(a, b):
    return lax.dot_general(a, b, (((1,), (1,)), ((), ())), preferred_element_type=jnp.float32)


def spread_kernel(group, arrays, *refs):
    ins, outs = refs[:arrays], refs[arrays:]
    me = lax.rem(lax.axis_index("sp"), group)
    order = class_major(ins[0].shape[0]).astype(jnp.bfloat16)
    for k in range(group):
        head = me ^ k
        cols = pl.ds(pl.multiple_of(head * HEAD_DIM, HEAD_DIM), HEAD_DIM)
        part = jnp.concatenate([ref[:, cols] for ref in ins], axis=1)
        outs[k][...] = dot(order, part).astype(jnp.bfloat16)


def spread(group, *arrays):
    rows = arrays[0].shape[0]
    out = jax.ShapeDtypeStruct((rows, HEAD_DIM * len(arrays)), jnp.bfloat16)
    return pl.pallas_call(
        functools.partial(spread_kernel, group, len(arrays)),
        out_shape=[out] * group,
        in_specs=[pl.BlockSpec(memory_space=pltpu.VMEM)] * len(arrays),
        out_specs=[pl.BlockSpec(memory_space=pltpu.VMEM)] * group,
        compiler_params=pltpu.CompilerParams(vmem_limit_bytes=VMEM_LIMIT),
        cost_estimate=pl.CostEstimate(flops=10**6, bytes_accessed=10**6, transcendentals=0),
    )(*arrays)


def far_bias(queries, keys, offset, valid):
    q_pos, k_pos = iota((queries, keys), 0), iota((queries, keys), 1) + offset
    near = jnp.abs(k_pos - q_pos) <= SIDE_KEY_COUNT
    return jnp.where(near & valid, 0.0, NEG)


def middle_place(row, per):
    quarter = FAR_DILATION // MIDDLE_DILATION
    return quarter * (row % per) + (row // per) % quarter


def token_place(row, per):
    return FAR_DILATION * (row % per) + row // per


def band(q_pos, k_pos):
    return jnp.where(jnp.abs(k_pos - q_pos) <= SIDE_KEY_COUNT, 0.0, NEG)


def pick_tokens(rows, start, count):
    column = token_place(iota((count, rows), 1), rows // FAR_DILATION)
    return jnp.where(column == iota((count, rows), 0) + start, 1.0, 0.0).astype(jnp.bfloat16)


def residue_rows(residue, per):
    quarter = FAR_DILATION // MIDDLE_DILATION
    return [pl.ds((MIDDLE_DILATION * s + residue) * per, per) for s in range(quarter)]


def softmax_parts(units):
    scores = [dot_t(q, k) + bias for q, k, _, bias in units]
    tops = [jnp.max(s, axis=1, keepdims=True) for s in scores]
    raised = [jnp.exp2((s - t) * EXP_SCALE).astype(jnp.bfloat16) for s, t in zip(scores, tops)]
    both = [
        dot(r, jnp.concatenate([v, jnp.ones_like(v)], axis=1))
        for r, (_, _, v, _) in zip(raised, units)
    ]
    return [
        (x[:, :HEAD_DIM], x[:, HEAD_DIM:], jnp.broadcast_to(t, (x.shape[0], HEAD_DIM)))
        for x, t in zip(both, tops)
    ]


def join(old, new):
    (num_a, den_a, top_a), (num_b, den_b, top_b) = old, new
    top = jnp.maximum(top_a, top_b)
    by_a, by_b = jnp.exp2((top_a - top) * EXP_SCALE), jnp.exp2((top_b - top) * EXP_SCALE)
    return num_a * by_a + num_b * by_b, den_a * by_a + den_b * by_b, top


def local_kernel(group, *refs):
    q_in, kv_in = refs[:group], refs[group : 2 * group]
    q_s, num_s, den_s, top_s = refs[2 * group : 2 * group + 4]
    kv_s, bias1, sems = refs[2 * group + 4 :]
    rows = q_s.shape[1]
    per = rows // FAR_DILATION
    quarter = FAR_DILATION // MIDDLE_DILATION
    part = per * quarter
    side = SIDE_KEY_COUNT
    me = lax.rem(lax.axis_index("sp"), group)
    stats = (num_s, den_s, top_s)

    copies = []
    for k in range(group):
        copies.append(pltpu.make_async_copy(q_in[k], q_s.at[me ^ k], sems.at[k]))
        copies.append(pltpu.make_async_copy(kv_in[k], kv_s.at[me ^ k], sems.at[group + k]))
    for copy in copies:
        copy.start()

    far = far_bias(group * per, group * per, 0, True)
    q_pos = middle_place(iota((part, 3 * part), 0), per)
    column = iota((part, 3 * part), 1)
    middle = band(q_pos, middle_place(column, per) + (column // part - 1) * part)
    q_pos = token_place(iota((rows, rows), 0), per)
    bias1[:, :rows] = band(q_pos, token_place(iota((rows, rows), 1), per))
    q_pos, column = token_place(iota((rows, 2 * side), 0), per), iota((rows, 2 * side), 1)
    bias1[:, rows:] = band(q_pos, jnp.where(column < side, column - side, rows + column - side))
    tails, heads = pick_tokens(rows, rows - side, side), pick_tokens(rows, 0, side)

    for copy in copies:
        copy.wait()

    batch = 8
    for first in range(0, FAR_DILATION, batch):
        ats = [pl.ds(c * per, per) for c in range(first, first + batch)]
        units = []
        for at in ats:
            q = q_s[:, at, :].reshape(group * per, HEAD_DIM)
            kv = kv_s[:, at, :].reshape(group * per, 2 * HEAD_DIM)
            units.append((q, kv[:, :HEAD_DIM], kv[:, HEAD_DIM:], far))
        for at, found in zip(ats, softmax_parts(units)):
            for ref, value in zip(stats, found):
                ref[:, at, :] = value.reshape(group, per, HEAD_DIM)

    for b in range(group):
        low, high = max(b - 1, 0), min(b + 2, group)
        columns = slice((low - b + 1) * part, (high - b + 1) * part)
        units, places = [], []
        for residue in range(MIDDLE_DILATION):
            ats = residue_rows(residue, per)
            q = jnp.concatenate([q_s[b, at, :] for at in ats], axis=0)
            kv = jnp.concatenate([kv_s[j, at, :] for j in range(low, high) for at in ats], axis=0)
            units.append((q, kv[:, :HEAD_DIM], kv[:, HEAD_DIM:], middle[:, columns]))
            places.append(ats)
        for ats, found in zip(places, softmax_parts(units)):
            old = [jnp.concatenate([ref[b, at, :] for at in ats], axis=0) for ref in stats]
            for ref, value in zip(stats, join(old, found)):
                for s, at in enumerate(ats):
                    ref[b, at, :] = value[s * per : (s + 1) * per]

    half = rows // 2
    for b in range(group):
        pieces, biases = [kv_s[b]], [bias1[:, :rows]]
        if b > 0:
            pieces.append(dot(tails, kv_s[b - 1]).astype(jnp.bfloat16))
        if b < group - 1:
            pieces.append(dot(heads, kv_s[b + 1]).astype(jnp.bfloat16))
        kv = jnp.concatenate(pieces, axis=0)
        low = rows if b > 0 else rows + side
        bias = jnp.concatenate([bias1[:, :rows], bias1[:, low : low + kv.shape[0] - rows]], axis=1)
        units = [
            (q_s[b, pl.ds(p * half, half), :], kv[:, :HEAD_DIM], kv[:, HEAD_DIM:], bias[p * half : (p + 1) * half])
            for p in range(2)
        ]
        for p, found in enumerate(softmax_parts(units)):
            at = pl.ds(p * half, half)
            for ref, value in zip(stats, join([ref[b, at, :] for ref in stats], found)):
                ref[b, at, :] = value


def halo_kernel(group, groups, *refs):
    q_in, num_in, den_in, top_in = refs[:4]
    kv_in, outs = refs[4 : 4 + 2 * group], refs[4 + 2 * group : 4 + 3 * group]
    q_s, num_s, den_s, top_s, kv_s, out_s, sems = refs[4 + 3 * group :]
    rows = q_s.shape[1]
    per = rows // FAR_DILATION
    quarter = FAR_DILATION // MIDDLE_DILATION
    part = per * quarter
    side = SIDE_KEY_COUNT
    here = lax.axis_index("sp")
    me, mine = lax.rem(here, group), here // group
    even = lax.rem(mine, 2) == 0
    has_before, has_after = mine > 0, mine < groups - 1
    stats = (num_s, den_s, top_s)

    copies = []
    for j, (source, target) in enumerate(zip((q_in, num_in, den_in, top_in), (q_s,) + stats)):
        copies.append(pltpu.make_async_copy(source, target, sems.at[j]))
    for j, base in enumerate((jnp.where(even, group, 0), jnp.where(even, 0, group))):
        for k in range(group):
            slot = kv_s.at[base + (me ^ k)]
            copies.append(pltpu.make_async_copy(kv_in[j * group + k], slot, sems.at[4 + j * group + k]))
    for copy in copies:
        copy.start()

    steps = group * per
    far = jnp.concatenate(
        [far_bias(steps, steps, -steps, has_before), far_bias(steps, steps, steps, has_after)], axis=1
    )
    column = iota((part, part), 1)
    q_mid, k_mid = middle_place(iota((part, part), 0), per), middle_place(column, per)
    before = jnp.where(has_before, band(q_mid, k_mid - part), NEG)
    after = jnp.where(has_after, band(q_mid, k_mid + part), NEG)
    near = []
    for residue in range(MIDDLE_DILATION):
        row, token = iota((part, side), 0), iota((part, side), 1)
        q_pos = FAR_DILATION * (row % per) + MIDDLE_DILATION * (row // per) + residue
        near.append(
            (
                jnp.where(has_before, band(q_pos, token - side), NEG),
                jnp.where(has_after, band(q_pos, token + rows), NEG),
            )
        )
    tails, heads = pick_tokens(rows, rows - side, side), pick_tokens(rows, 0, side)
    natural = token_order(rows).astype(jnp.bfloat16)

    for copy in copies:
        copy.wait()

    tail = dot(tails, kv_s[group - 1]).astype(jnp.bfloat16)
    head = dot(heads, kv_s[group]).astype(jnp.bfloat16)
    units, places = [], []
    for b, slot, ends, mid, which in ((0, group - 1, tail, before, 0), (group - 1, group, head, after, 1)):
        for residue in range(MIDDLE_DILATION):
            ats = residue_rows(residue, per)
            q = jnp.concatenate([q_s[b, at, :] for at in ats], axis=0)
            kv = jnp.concatenate([kv_s[slot, at, :] for at in ats] + [ends], axis=0)
            bias = jnp.concatenate([mid, near[residue][which]], axis=1)
            units.append((q, kv[:, :HEAD_DIM], kv[:, HEAD_DIM:], bias))
            places.append((b, ats))
    for (b, ats), found in zip(places, softmax_parts(units)):
        old = [jnp.concatenate([ref[b, at, :] for at in ats], axis=0) for ref in stats]
        for ref, value in zip(stats, join(old, found)):
            for s, at in enumerate(ats):
                ref[b, at, :] = value[s * per : (s + 1) * per]

    batch = 8
    for first in range(0, FAR_DILATION, batch):
        ats = [pl.ds(c * per, per) for c in range(first, first + batch)]
        units = []
        for at in ats:
            q = q_s[:, at, :].reshape(steps, HEAD_DIM)
            kv = kv_s[:, at, :].reshape(2 * steps, 2 * HEAD_DIM)
            units.append((q, kv[:, :HEAD_DIM], kv[:, HEAD_DIM:], far))
        for at, found in zip(ats, softmax_parts(units)):
            old = [ref[:, at, :].reshape(steps, HEAD_DIM) for ref in stats]
            num, den, _ = join(old, found)
            out_s[:, at, :] = (num / den).astype(jnp.bfloat16).reshape(group, per, HEAD_DIM)
    for k in range(group):
        outs[k][...] = dot(natural, out_s[me ^ k]).astype(jnp.bfloat16)


def attend_local(group, q, own):
    rows = q[0].shape[0]
    f32, bf16 = jnp.float32, jnp.bfloat16
    shape = (group, rows, HEAD_DIM)
    return pl.pallas_call(
        functools.partial(local_kernel, group),
        out_shape=[jax.ShapeDtypeStruct(shape, kind) for kind in (bf16, f32, f32, f32)],
        in_specs=[pl.BlockSpec(memory_space=pl.ANY)] * (2 * group),
        out_specs=[pl.BlockSpec(memory_space=pltpu.VMEM)] * 4,
        scratch_shapes=[
            pltpu.VMEM((group, rows, 2 * HEAD_DIM), bf16),
            pltpu.VMEM((rows, rows + 2 * SIDE_KEY_COUNT), f32),
            pltpu.SemaphoreType.DMA((2 * group,)),
        ],
        compiler_params=pltpu.CompilerParams(vmem_limit_bytes=VMEM_LIMIT),
        cost_estimate=pl.CostEstimate(flops=LOCAL_FLOPS, bytes_accessed=10**6, transcendentals=0),
    )(*q, *own)


def attend_halo(group, groups, found, even, odd):
    q = found[0]
    rows = q.shape[1]
    f32, bf16 = jnp.float32, jnp.bfloat16
    shape = (group, rows, HEAD_DIM)
    return pl.pallas_call(
        functools.partial(halo_kernel, group, groups),
        out_shape=[jax.ShapeDtypeStruct((rows, HEAD_DIM), bf16)] * group,
        in_specs=[pl.BlockSpec(memory_space=pl.ANY)] * (4 + 2 * group),
        out_specs=[pl.BlockSpec(memory_space=pltpu.VMEM)] * group,
        scratch_shapes=[
            pltpu.VMEM(shape, bf16),
            pltpu.VMEM(shape, f32),
            pltpu.VMEM(shape, f32),
            pltpu.VMEM(shape, f32),
            pltpu.VMEM((2 * group, rows, 2 * HEAD_DIM), bf16),
            pltpu.VMEM(shape, bf16),
            pltpu.SemaphoreType.DMA((4 + 2 * group,)),
        ],
        compiler_params=pltpu.CompilerParams(vmem_limit_bytes=VMEM_LIMIT),
        cost_estimate=pl.CostEstimate(flops=10**9, bytes_accessed=10**6, transcendentals=0),
    )(*found, *even, *odd)


def project_kernel(group, *refs):
    own, other = refs[:group], refs[group : 2 * group]
    w_ref, out_ref = refs[2 * group :]
    me, side = lax.rem(lax.axis_index("sp"), group), lax.axis_index("tp")
    total = None
    for k in range(group):
        left = jnp.concatenate([own[k][...], other[k][...]], axis=1)
        right = []
        for core in (side, 1 - side):
            row = (core * group + (me ^ k)) * HEAD_DIM
            right.append(w_ref[pl.ds(pl.multiple_of(row, HEAD_DIM), HEAD_DIM), :])
        term = dot(left, jnp.concatenate(right, axis=0))
        total = term if total is None else total + term
    out_ref[...] = total.astype(jnp.bfloat16)


def project(group, own, other, w_out):
    rows, width = own[0].shape[0], w_out.shape[1]
    return pl.pallas_call(
        functools.partial(project_kernel, group),
        out_shape=jax.ShapeDtypeStruct((rows, width), jnp.bfloat16),
        in_specs=[pl.BlockSpec(memory_space=pltpu.VMEM)] * (2 * group + 1),
        out_specs=pl.BlockSpec(memory_space=pltpu.VMEM),
        compiler_params=pltpu.CompilerParams(vmem_limit_bytes=VMEM_LIMIT),
        cost_estimate=pl.CostEstimate(flops=10**9, bytes_accessed=10**6, transcendentals=0),
    )(*own, *other, w_out)


def per_device(queries, keys, values, w_out):
    rows = queries.shape[0]
    shards = lax.axis_size("sp")
    group = -(-(SIDE_KEY_COUNT * FAR_DILATION) // rows)
    groups = shards // group

    def inside(value, k):
        return lax.ppermute(value, "sp", [(s, s ^ k) for s in range(shards)])

    def across(value, parity):
        pairs = []
        for s in range(shards):
            mine = s // group
            beside = mine + 1 if mine % 2 == parity else mine - 1
            for t in range(2):
                if 0 <= beside < groups:
                    pairs.append((2 * s + t, 2 * (s + (beside - mine) * group) + t))
                else:
                    pairs.append((2 * s + t, 2 * s + 1 - t))
        return lax.ppermute(value, ("sp", "tp"), pairs)

    def other_core(value):
        return lax.ppermute(value, "tp", [(0, 1), (1, 0)])

    kv = spread(group, keys, values)
    q = spread(group, queries)
    own = [kv[0]] + [inside(kv[k], k) for k in range(1, group)]
    even = [across(piece, 0) for piece in own]
    odd = [across(piece, 1) for piece in own]
    q = [q[0]] + [inside(q[k], k) for k in range(1, group)]
    out = attend_halo(group, groups, attend_local(group, q, own), even, odd)
    out = [out[0]] + [inside(out[k], k) for k in range(1, group)]
    return project(group, out, [other_core(piece) for piece in out], w_out)


def solution(mesh):
    in_specs = (P("sp", "tp"), P("sp", "tp"), P("sp", "tp"), P(None, "tp"))
    out_specs = P("sp", "tp")
    return jax.shard_map(
        per_device, mesh=mesh, in_specs=in_specs, out_specs=out_specs, check_vma=False
    )
```

time: 58.8 us -> 44.5 us (0.76)
  Pallas kernels: 21.8 us -> 10.6 us
  waiting for transfers between devices: 15.9 us -> 10.1 us
  local copies, waits for them, and re-layouts: 1.23 us -> 2.85 us
  starting transfers between devices: 19.4 us -> 20.7 us
    pallas_call x1 -> x2, Pallas kernels: 13.6 us -> 8.46 us  [the longest x1 4.92 us: attend_local(): pl.pallas_call(functools.partial(local_kernel, group), out_shape=[jax.Sha...]
    ppermute x8, waiting for transfers between devices: 5.38 us -> 0.59 us  [across(): return lax.ppermute(value, ('sp', 'tp'), pairs)]
    pallas_call x2, Pallas kernels: 3.97 us -> 0.61 us  [spread(): pl.pallas_call(functools.partial(spread_kernel, group, len(arrays)), out_...]
    pallas_call x1, Pallas kernels: 4.2 us -> 1.5 us  [project(): pl.pallas_call(functools.partial(project_kernel, group), out_shape=jax.Sh...]
    unnamed x42 -> x8, local copies, waits for them, and re-layouts: 1.23 us -> 2.85 us
    ppermute x9, starting transfers between devices: 12.5 us -> 13.6 us  [inside(): return lax.ppermute(value, 'sp', [(s, s ^ k) for s in range(shards)])]
    ppermute x9, waiting for transfers between devices: 9.29 us -> 8.23 us  [inside(): return lax.ppermute(value, 'sp', [(s, s ^ k) for s in range(shards)])]
  transfers between devices with their start and end apart: 21 -> 21, of which waited for: 8 -> 7; matrix products, arithmetic and copies ran while one was open for 0% -> 0% of each run, Pallas kernels for 3% -> 12%
where the time goes in v2:
time: 44.5 us; the launch traced here: 44.3 us
  starting transfers between devices  20.7 us (47%)
  Pallas kernels  10.6 us (24%)
  waiting for transfers between devices  10.1 us (23%)
  local copies, waits for them, and re-layouts  2.85 us (6%)
    ppermute x9, starting transfers between devices, inside(): return lax.ppermute(value, 'sp', [(s, s ^ k) for s in range(shards)])  13.6 us
    ppermute x9, waiting for transfers between devices, inside(): return lax.ppermute(value, 'sp', [(s, s ^ k) for s in range(shards)])  8.23 us
    ppermute x8, starting transfers between devices, across(): return lax.ppermute(value, ('sp', 'tp'), pairs)  7.11 us
    pallas_call x1, Pallas kernels, attend_local(): pl.pallas_call(functools.partial(local_kernel, group), out_shape=[jax.Sha...  4.92 us
    pallas_call x1, Pallas kernels, attend_halo(): pl.pallas_call(functools.partial(halo_kernel, group, groups), out_shape=[...  3.54 us
    unnamed x8, local copies, waits for them, and re-layouts  2.85 us
    pallas_call x1, Pallas kernels, project(): pl.pallas_call(functools.partial(project_kernel, group), out_shape=jax.Sh...  1.5 us
    ppermute x4, waiting for transfers between devices, other_core(): return lax.ppermute(value, 'tp', [(0, 1), (1, 0)])  1.24 us
  transfers between devices with their start and end apart: 21, of which 7 were waited for; matrix products, arithmetic and copies ran while one was open for 0% of the time, Pallas kernels for 12%

profile of v2, /device:TPU:0, one launch (start us, length us, event | category | flops | bytes accessed | tf_op | source)
XLA Modules:
  0.0 44.3 jit_solution(7186244390875010524)
XLA Ops:
  0.0 0.0 copy-start
  0.0 0.9 %copy-done = bf16[256,512]{1,0:T(8,128)(2,1)S(1)} copy-done((bf16[256,512]{1,0:T(8,128)(2,1)S(1)}, bf16[256,512]{1,0:T(8,128)(2,1)}, u32[]{:S(2)}) %copy-start) | copy-done | bytes 262168
  1.0 0.0 copy-start.1
  1.0 0.9 %copy-done.1 = bf16[256,512]{1,0:T(8,128)(2,1)S(1)} copy-done((bf16[256,512]{1,0:T(8,128)(2,1)S(1)}, bf16[256,512]{1,0:T(8,128)(2,1)}, u32[]{:S(2)}) %copy-start.1) | copy-done | bytes 262168
  1.9 0.3 shard_map.47
  2.2 3.0 %collective-permute-start.3 = (bf16[256,256]{1,0:T(8,128)(2,1)S(1)}, bf16[256,256]{1,0:T(8,128)(2,1)S(1)}, u32[]{:S(2)}, u32[]{:S(2)}) collective-permute-start(bf16[256,256]{1,0:T(8,128)(2,1)S(1)} %get-tuple-element.26), channel_id=1, source_target_pairs={{0,2},{2,0},{4,6},{6,4},{8,10},{10,8},{12,14},{14,12},{16,18},{18,... | collective-permute-start | bytes 393224 | tf_op jit(solution)/shard_map/ppermute | solution.py:359
  5.3 0.0 copy-start.2
  5.3 0.9 %copy-done.2 = bf16[256,512]{1,0:T(8,128)(2,1)S(1)} copy-done((bf16[256,512]{1,0:T(8,128)(2,1)S(1)}, bf16[256,512]{1,0:T(8,128)(2,1)}, u32[]{:S(2)}) %copy-start.2) | copy-done | bytes 262168
  6.2 0.3 shard_map.46
  6.5 0.1 collective-permute-start
  6.6 2.0 %collective-permute-start.1 = (bf16[256,128]{1,0:T(8,128)(2,1)S(1)}, bf16[256,128]{1,0:T(8,128)(2,1)S(1)}, u32[]{:S(2)}, u32[]{:S(2)}) collective-permute-start(bf16[256,128]{1,0:T(8,128)(2,1)S(1)} %get-tuple-element.23), channel_id=1, source_target_pairs={{0,4},{2,6},{4,0},{6,2},{8,12},{10,14},{12,8},{14,10},{16,20},{18,... | collective-permute-start | bytes 196616 | tf_op jit(solution)/shard_map/ppermute | solution.py:359
  8.6 1.4 %collective-permute-start.2 = (bf16[256,128]{1,0:T(8,128)(2,1)S(1)}, bf16[256,128]{1,0:T(8,128)(2,1)S(1)}, u32[]{:S(2)}, u32[]{:S(2)}) collective-permute-start(bf16[256,128]{1,0:T(8,128)(2,1)S(1)} %get-tuple-element.24), channel_id=1, source_target_pairs={{0,6},{2,4},{4,2},{6,0},{8,14},{10,12},{12,10},{14,8},{16,22},{18,... | collective-permute-start | bytes 196616 | tf_op jit(solution)/shard_map/ppermute | solution.py:359
  10.1 1.5 %collective-permute-start.4 = (bf16[256,256]{1,0:T(8,128)(2,1)S(1)}, bf16[256,256]{1,0:T(8,128)(2,1)S(1)}, u32[]{:S(2)}, u32[]{:S(2)}) collective-permute-start(bf16[256,256]{1,0:T(8,128)(2,1)S(1)} %get-tuple-element.27), channel_id=1, source_target_pairs={{0,4},{2,6},{4,0},{6,2},{8,12},{10,14},{12,8},{14,10},{16,20},{18,... | collective-permute-start | bytes 393224 | tf_op jit(solution)/shard_map/ppermute | solution.py:359
  11.6 0.0 collective-permute-done.refs_1_
  11.6 1.5 %collective-permute-start.5 = (bf16[256,256]{1,0:T(8,128)(2,1)S(1)}, bf16[256,256]{1,0:T(8,128)(2,1)S(1)}, u32[]{:S(2)}, u32[]{:S(2)}) collective-permute-start(bf16[256,256]{1,0:T(8,128)(2,1)S(1)} %get-tuple-element.28), channel_id=1, source_target_pairs={{0,6},{2,4},{4,2},{6,0},{8,14},{10,12},{12,10},{14,8},{16,22},{18,... | collective-permute-start | bytes 393224 | tf_op jit(solution)/shard_map/ppermute | solution.py:359
  13.1 0.0 collective-permute-done.1.refs_2_
  13.1 0.0 collective-permute-start.10
  13.1 1.1 %collective-permute-done.2.refs_3_ = bf16[256,128]{1,0:T(8,128)(2,1)S(1)} collective-permute-done((bf16[256,128]{1,0:T(8,128)(2,1)S(1)}, bf16[256,128]{1,0:T(8,128)(2,1)S(1)}, u32[]{:S(2)}, u32[]{:S(2)}) %collective-permute-start.2) | collective-permute-done | bytes 65568 | tf_op jit(solution)/shard_map/ppermute | solution.py:359
  14.2 2.1 %collective-permute-start.6 = (bf16[256,256]{1,0:T(8,128)(2,1)S(1)}, bf16[256,256]{1,0:T(8,128)(2,1)S(1)}, u32[]{:S(2)}, u32[]{:S(2)}) collective-permute-start(bf16[256,256]{1,0:T(8,128)(2,1)S(1)} %get-tuple-element.25.refs_4_), channel_id=1, source_target_pairs={{0,8},{1,9},{2,10},{3,11},{4,12},{5,13},{6,14},{7,15},{8,0},{9,1},... | collective-permute-start | bytes 393224 | tf_op jit(solution)/shard_map/ppermute | solution.py:371
  16.3 0.0 collective-permute-done.3.refs_5_
  16.3 0.0 collective-permute-start.11
  16.3 2.0 %collective-permute-done.4.refs_6_ = bf16[256,256]{1,0:T(8,128)(2,1)S(1)} collective-permute-done((bf16[256,256]{1,0:T(8,128)(2,1)S(1)}, bf16[256,256]{1,0:T(8,128)(2,1)S(1)}, u32[]{:S(2)}, u32[]{:S(2)}) %collective-permute-start.4) | collective-permute-done | bytes 131104 | tf_op jit(solution)/shard_map/ppermute | solution.py:359
  18.3 1.7 %collective-permute-start.7 = (bf16[256,256]{1,0:T(8,128)(2,1)S(1)}, bf16[256,256]{1,0:T(8,128)(2,1)S(1)}, u32[]{:S(2)}, u32[]{:S(2)}) collective-permute-start(bf16[256,256]{1,0:T(8,128)(2,1)S(1)} %collective-permute-done.3.refs_5_), channel_id=1, source_target_pairs={{0,8},{1,9},{2,10},{3,11},{4,12},{5,13},{6,14},{7,15},{8,0},{9,1},... | collective-permute-start | bytes 393224 | tf_op jit(solution)/shard_map/ppermute | solution.py:371
  20.0 0.0 collective-permute-done.5.refs_7_
  20.0 0.0 collective-permute-start.12
  20.0 0.0 collective-permute-done.10.refs_8_
  20.0 0.5 %collective-permute-start.13 = (bf16[256,256]{1,0:T(8,128)(2,1)S(1)}, bf16[256,256]{1,0:T(8,128)(2,1)S(1)}, u32[]{:S(2)}, u32[]{:S(2)}) collective-permute-start(bf16[256,256]{1,0:T(8,128)(2,1)S(1)} %collective-permute-done.5.refs_7_), channel_id=1, source_target_pairs={{0,1},{1,0},{2,3},{3,2},{4,5},{5,4},{6,7},{7,6},{8,16},{9,17},{10,... | collective-permute-start | bytes 393224 | tf_op jit(solution)/shard_map/ppermute | solution.py:371
  20.5 0.0 collective-permute-done.6.refs_4_
  20.5 2.7 %collective-permute-start.8 = (bf16[256,256]{1,0:T(8,128)(2,1)S(1)}, bf16[256,256]{1,0:T(8,128)(2,1)S(1)}, u32[]{:S(2)}, u32[]{:S(2)}) collective-permute-start(bf16[256,256]{1,0:T(8,128)(2,1)S(1)} %collective-permute-done.4.refs_6_), channel_id=1, source_target_pairs={{0,8},{1,9},{2,10},{3,11},{4,12},{5,13},{6,14},{7,15},{8,0},{9,1},... | collective-permute-start | bytes 393224 | tf_op jit(solution)/shard_map/ppermute | solution.py:371
  23.2 0.0 collective-permute-done.11.refs_9_
  23.2 0.1 collective-permute-start.9
  23.3 4.9 %shard_map.48 = (bf16[4,256,128]{2,1,0:T(8,128)(2,1)S(1)}, f32[4,256,128]{2,1,0:T(8,128)S(1)}, f32[4,256,128]{2,1,0:T(8,128)S(1)}, f32[4,256,128]{2,1,0:T(8,128)S(1)}) custom-call(bf16[256,128]{1,0:T(8,128)(2,1)S(1)} %get-tuple-element.21.refs_0_, bf16[256,128]{1,0:T(8,128)(2,1)S(1)} %collective-permute-done.refs_1_, ...), custom_call_target="tpu_custom_call" | custom-call | flops 1000000000 | bytes 1000000 | tf_op jit(solution)/shard_map/pallas_call | solution.py:285
  28.2 0.0 copy-start.3
  28.2 0.0 collective-permute-done.12.refs_10_
  28.2 0.0 collective-permute-done.13.refs_11_
  28.3 0.0 collective-permute-done.7.refs_5_
  28.3 0.0 collective-permute-done.8.refs_6_
  28.3 0.6 %collective-permute-done.9.refs_7_ = bf16[256,256]{1,0:T(8,128)(2,1)S(1)} collective-permute-done((bf16[256,256]{1,0:T(8,128)(2,1)S(1)}, bf16[256,256]{1,0:T(8,128)(2,1)S(1)}, u32[]{:S(2)}, u32[]{:S(2)}) %collective-permute-start.9) | collective-permute-done | bytes 131104 | tf_op jit(solution)/shard_map/ppermute | solution.py:371
  28.8 3.5 %shard_map.49 = (bf16[256,128]{1,0:T(8,128)(2,1)S(1)}, bf16[256,128]{1,0:T(8,128)(2,1)S(1)}, bf16[256,128]{1,0:T(8,128)(2,1)S(1)}, bf16[256,128]{1,0:T(8,128)(2,1)S(1)}) custom-call(bf16[4,256,128]{2,1,0:T(8,128)(2,1)S(1)} %get-tuple-element.29.refs_0_, f32[4,256,128]{2,1,0:T(8,128)S(1)} %get-tuple-element.30.refs_1_, ...), custom_call_target="tpu_custom_call" | custom-call | flops 1000000000 | bytes 1000000 | tf_op jit(solution)/shard_map/pallas_call | solution.py:305
  32.4 1.3 %collective-permute-start.14 = (bf16[256,128]{1,0:T(8,128)(2,1)S(1)}, bf16[256,128]{1,0:T(8,128)(2,1)S(1)}, u32[]{:S(2)}, u32[]{:S(2)}) collective-permute-start(bf16[256,128]{1,0:T(8,128)(2,1)S(1)} %get-tuple-element.34), channel_id=1, source_target_pairs={{0,2},{2,0},{4,6},{6,4},{8,10},{10,8},{12,14},{14,12},{16,18},{18,... | collective-permute-start | bytes 196616 | tf_op jit(solution)/shard_map/ppermute | solution.py:359
  33.7 2.7 %collective-permute-start.15 = (bf16[256,128]{1,0:T(8,128)(2,1)S(1)}, bf16[256,128]{1,0:T(8,128)(2,1)S(1)}, u32[]{:S(2)}, u32[]{:S(2)}) collective-permute-start(bf16[256,128]{1,0:T(8,128)(2,1)S(1)} %get-tuple-element.35), channel_id=1, source_target_pairs={{0,4},{2,6},{4,0},{6,2},{8,12},{10,14},{12,8},{14,10},{16,20},{18,... | collective-permute-start | bytes 196616 | tf_op jit(solution)/shard_map/ppermute | solution.py:359
  36.4 0.0 collective-permute-start.16
  36.4 0.0 collective-permute-start.17
  36.4 0.6 %collective-permute-done.14.refs_1_ = bf16[256,128]{1,0:T(8,128)(2,1)S(1)} collective-permute-done((bf16[256,128]{1,0:T(8,128)(2,1)S(1)}, bf16[256,128]{1,0:T(8,128)(2,1)S(1)}, u32[]{:S(2)}, u32[]{:S(2)}) %collective-permute-start.14) | collective-permute-done | bytes 65568 | tf_op jit(solution)/shard_map/ppermute | solution.py:359
  37.0 0.0 collective-permute-start.18
  37.0 2.2 %collective-permute-done.15.refs_2_ = bf16[256,128]{1,0:T(8,128)(2,1)S(1)} collective-permute-done((bf16[256,128]{1,0:T(8,128)(2,1)S(1)}, bf16[256,128]{1,0:T(8,128)(2,1)S(1)}, u32[]{:S(2)}, u32[]{:S(2)}) %collective-permute-start.15) | collective-permute-done | bytes 65568 | tf_op jit(solution)/shard_map/ppermute | solution.py:359
  39.2 0.0 collective-permute-start.19
  39.2 2.3 %collective-permute-done.16.refs_3_ = bf16[256,128]{1,0:T(8,128)(2,1)S(1)} collective-permute-done((bf16[256,128]{1,0:T(8,128)(2,1)S(1)}, bf16[256,128]{1,0:T(8,128)(2,1)S(1)}, u32[]{:S(2)}, u32[]{:S(2)}) %collective-permute-start.16) | collective-permute-done | bytes 65568 | tf_op jit(solution)/shard_map/ppermute | solution.py:359
  41.5 0.0 collective-permute-start.20
  41.5 0.0 collective-permute-done.17.refs_4_
  41.5 0.0 collective-permute-done.18.refs_5_
  41.5 0.0 collective-permute-done.19.refs_6_
  41.5 1.2 %collective-permute-done.20.refs_7_ = bf16[256,128]{1,0:T(8,128)(2,1)S(1)} collective-permute-done((bf16[256,128]{1,0:T(8,128)(2,1)S(1)}, bf16[256,128]{1,0:T(8,128)(2,1)S(1)}, u32[]{:S(2)}, u32[]{:S(2)}) %collective-permute-start.20) | collective-permute-done | bytes 65568 | tf_op jit(solution)/shard_map/ppermute | solution.py:374
  42.8 0.0 copy-done.3
  42.8 1.5 %shard_map.50 = bf16[256,1024]{1,0:T(8,128)(2,1)} custom-call(bf16[256,128]{1,0:T(8,128)(2,1)S(1)} %get-tuple-element.33.refs_0_, bf16[256,128]{1,0:T(8,128)(2,1)S(1)} %collective-permute-done.14.refs_1_, bf16[256,128]{1,0:T(8,128)(2,1)S(1)} %collective-permute-done.15.refs_2_, bf16[256,128]{1,0:T(8,128)(2,1)S(1)} %collective-permute-done.16.refs_3_, ...), custom_call_target="tpu_custom_call" | custom-call | flops 1000000000 | bytes 1000000 | tf_op jit(solution)/shard_map/pallas_call | solution.py:342
Async XLA Ops:
  0.0 0.9 %copy-start = (bf16[256,512]{1,0:T(8,128)(2,1)S(1)}, bf16[256,512]{1,0:T(8,128)(2,1)}, u32[]{:S(2)}) copy-start(bf16[256,512]{1,0:T(8,128)(2,1)} %refs_0_.3) | copy-start | bytes 786436
  1.0 0.9 %copy-start.1 = (bf16[256,512]{1,0:T(8,128)(2,1)S(1)}, bf16[256,512]{1,0:T(8,128)(2,1)}, u32[]{:S(2)}) copy-start(bf16[256,512]{1,0:T(8,128)(2,1)} %refs_1_.1) | copy-start | bytes 786436
  2.2 14.0 %collective-permute-start.3 = (bf16[256,256]{1,0:T(8,128)(2,1)S(1)}, bf16[256,256]{1,0:T(8,128)(2,1)S(1)}, u32[]{:S(2)}, u32[]{:S(2)}) collective-permute-start(bf16[256,256]{1,0:T(8,128)(2,1)S(1)} %get-tuple-element.26), channel_id=1, source_target_pairs={{0,2},{2,0},{4,6},{6,4},{8,10},{10,8},{12,14},{14,12},{16,18},{18,... | collective-permute-start | bytes 393224 | tf_op jit(solution)/shard_map/ppermute | solution.py:359
  5.3 0.9 %copy-start.2 = (bf16[256,512]{1,0:T(8,128)(2,1)S(1)}, bf16[256,512]{1,0:T(8,128)(2,1)}, u32[]{:S(2)}) copy-start(bf16[256,512]{1,0:T(8,128)(2,1)} %refs_0_.2) | copy-start | bytes 786436
  6.5 5.1 %collective-permute-start = (bf16[256,128]{1,0:T(8,128)(2,1)S(1)}, bf16[256,128]{1,0:T(8,128)(2,1)S(1)}, u32[]{:S(2)}, u32[]{:S(2)}) collective-permute-start(bf16[256,128]{1,0:T(8,128)(2,1)S(1)} %get-tuple-element.22), channel_id=1, source_target_pairs={{0,2},{2,0},{4,6},{6,4},{8,10},{10,8},{12,14},{14,12},{16,18},{18,... | collective-permute-start | bytes 196616 | tf_op jit(solution)/shard_map/ppermute | solution.py:359
  6.6 6.5 %collective-permute-start.1 = (bf16[256,128]{1,0:T(8,128)(2,1)S(1)}, bf16[256,128]{1,0:T(8,128)(2,1)S(1)}, u32[]{:S(2)}, u32[]{:S(2)}) collective-permute-start(bf16[256,128]{1,0:T(8,128)(2,1)S(1)} %get-tuple-element.23), channel_id=1, source_target_pairs={{0,4},{2,6},{4,0},{6,2},{8,12},{10,14},{12,8},{14,10},{16,20},{18,... | collective-permute-start | bytes 196616 | tf_op jit(solution)/shard_map/ppermute | solution.py:359
  8.6 5.5 %collective-permute-start.2 = (bf16[256,128]{1,0:T(8,128)(2,1)S(1)}, bf16[256,128]{1,0:T(8,128)(2,1)S(1)}, u32[]{:S(2)}, u32[]{:S(2)}) collective-permute-start(bf16[256,128]{1,0:T(8,128)(2,1)S(1)} %get-tuple-element.24), channel_id=1, source_target_pairs={{0,6},{2,4},{4,2},{6,0},{8,14},{10,12},{12,10},{14,8},{16,22},{18,... | collective-permute-start | bytes 196616 | tf_op jit(solution)/shard_map/ppermute | solution.py:359
  10.1 8.2 %collective-permute-start.4 = (bf16[256,256]{1,0:T(8,128)(2,1)S(1)}, bf16[256,256]{1,0:T(8,128)(2,1)S(1)}, u32[]{:S(2)}, u32[]{:S(2)}) collective-permute-start(bf16[256,256]{1,0:T(8,128)(2,1)S(1)} %get-tuple-element.27), channel_id=1, source_target_pairs={{0,4},{2,6},{4,0},{6,2},{8,12},{10,14},{12,8},{14,10},{16,20},{18,... | collective-permute-start | bytes 393224 | tf_op jit(solution)/shard_map/ppermute | solution.py:359
  11.6 8.4 %collective-permute-start.5 = (bf16[256,256]{1,0:T(8,128)(2,1)S(1)}, bf16[256,256]{1,0:T(8,128)(2,1)S(1)}, u32[]{:S(2)}, u32[]{:S(2)}) collective-permute-start(bf16[256,256]{1,0:T(8,128)(2,1)S(1)} %get-tuple-element.28), channel_id=1, source_target_pairs={{0,6},{2,4},{4,2},{6,0},{8,14},{10,12},{12,10},{14,8},{16,22},{18,... | collective-permute-start | bytes 393224 | tf_op jit(solution)/shard_map/ppermute | solution.py:359
  13.1 6.9 %collective-permute-start.10 = (bf16[256,256]{1,0:T(8,128)(2,1)S(1)}, bf16[256,256]{1,0:T(8,128)(2,1)S(1)}, u32[]{:S(2)}, u32[]{:S(2)}) collective-permute-start(bf16[256,256]{1,0:T(8,128)(2,1)S(1)} %get-tuple-element.25.refs_4_), channel_id=1, source_target_pairs={{0,1},{1,0},{2,3},{3,2},{4,5},{5,4},{6,7},{7,6},{8,16},{9,17},{10,... | collective-permute-start | bytes 393224 | tf_op jit(solution)/shard_map/ppermute | solution.py:371
  14.2 6.3 %collective-permute-start.6 = (bf16[256,256]{1,0:T(8,128)(2,1)S(1)}, bf16[256,256]{1,0:T(8,128)(2,1)S(1)}, u32[]{:S(2)}, u32[]{:S(2)}) collective-permute-start(bf16[256,256]{1,0:T(8,128)(2,1)S(1)} %get-tuple-element.25.refs_4_), channel_id=1, source_target_pairs={{0,8},{1,9},{2,10},{3,11},{4,12},{5,13},{6,14},{7,15},{8,0},{9,1},... | collective-permute-start | bytes 393224 | tf_op jit(solution)/shard_map/ppermute | solution.py:371
  16.3 7.0 %collective-permute-start.11 = (bf16[256,256]{1,0:T(8,128)(2,1)S(1)}, bf16[256,256]{1,0:T(8,128)(2,1)S(1)}, u32[]{:S(2)}, u32[]{:S(2)}) collective-permute-start(bf16[256,256]{1,0:T(8,128)(2,1)S(1)} %collective-permute-done.3.refs_5_), channel_id=1, source_target_pairs={{0,1},{1,0},{2,3},{3,2},{4,5},{5,4},{6,7},{7,6},{8,16},{9,17},{10,... | collective-permute-start | bytes 393224 | tf_op jit(solution)/shard_map/ppermute | solution.py:371
  18.3 10.0 %collective-permute-start.7 = (bf16[256,256]{1,0:T(8,128)(2,1)S(1)}, bf16[256,256]{1,0:T(8,128)(2,1)S(1)}, u32[]{:S(2)}, u32[]{:S(2)}) collective-permute-start(bf16[256,256]{1,0:T(8,128)(2,1)S(1)} %collective-permute-done.3.refs_5_), channel_id=1, source_target_pairs={{0,8},{1,9},{2,10},{3,11},{4,12},{5,13},{6,14},{7,15},{8,0},{9,1},... | collective-permute-start | bytes 393224 | tf_op jit(solution)/shard_map/ppermute | solution.py:371
  20.0 8.3 %collective-permute-start.12 = (bf16[256,256]{1,0:T(8,128)(2,1)S(1)}, bf16[256,256]{1,0:T(8,128)(2,1)S(1)}, u32[]{:S(2)}, u32[]{:S(2)}) collective-permute-start(bf16[256,256]{1,0:T(8,128)(2,1)S(1)} %collective-permute-done.4.refs_6_), channel_id=1, source_target_pairs={{0,1},{1,0},{2,3},{3,2},{4,5},{5,4},{6,7},{7,6},{8,16},{9,17},{10,... | collective-permute-start | bytes 393224 | tf_op jit(solution)/shard_map/ppermute | solution.py:371
  20.0 8.3 %collective-permute-start.13 = (bf16[256,256]{1,0:T(8,128)(2,1)S(1)}, bf16[256,256]{1,0:T(8,128)(2,1)S(1)}, u32[]{:S(2)}, u32[]{:S(2)}) collective-permute-start(bf16[256,256]{1,0:T(8,128)(2,1)S(1)} %collective-permute-done.5.refs_7_), channel_id=1, source_target_pairs={{0,1},{1,0},{2,3},{3,2},{4,5},{5,4},{6,7},{7,6},{8,16},{9,17},{10,... | collective-permute-start | bytes 393224 | tf_op jit(solution)/shard_map/ppermute | solution.py:371
  20.5 7.8 %collective-permute-start.8 = (bf16[256,256]{1,0:T(8,128)(2,1)S(1)}, bf16[256,256]{1,0:T(8,128)(2,1)S(1)}, u32[]{:S(2)}, u32[]{:S(2)}) collective-permute-start(bf16[256,256]{1,0:T(8,128)(2,1)S(1)} %collective-permute-done.4.refs_6_), channel_id=1, source_target_pairs={{0,8},{1,9},{2,10},{3,11},{4,12},{5,13},{6,14},{7,15},{8,0},{9,1},... | collective-permute-start | bytes 393224 | tf_op jit(solution)/shard_map/ppermute | solution.py:371
  23.2 5.6 %collective-permute-start.9 = (bf16[256,256]{1,0:T(8,128)(2,1)S(1)}, bf16[256,256]{1,0:T(8,128)(2,1)S(1)}, u32[]{:S(2)}, u32[]{:S(2)}) collective-permute-start(bf16[256,256]{1,0:T(8,128)(2,1)S(1)} %collective-permute-done.5.refs_7_), channel_id=1, source_target_pairs={{0,8},{1,9},{2,10},{3,11},{4,12},{5,13},{6,14},{7,15},{8,0},{9,1},... | collective-permute-start | bytes 393224 | tf_op jit(solution)/shard_map/ppermute | solution.py:371
  28.2 14.6 %copy-start.3 = (bf16[1024,1024]{1,0:T(8,128)(2,1)S(1)}, bf16[1024,1024]{1,0:T(8,128)(2,1)}, u32[]{:S(2)}) copy-start(bf16[1024,1024]{1,0:T(8,128)(2,1)} %refs_8_.1) | copy-start | bytes 6291460
  32.4 4.6 %collective-permute-start.14 = (bf16[256,128]{1,0:T(8,128)(2,1)S(1)}, bf16[256,128]{1,0:T(8,128)(2,1)S(1)}, u32[]{:S(2)}, u32[]{:S(2)}) collective-permute-start(bf16[256,128]{1,0:T(8,128)(2,1)S(1)} %get-tuple-element.34), channel_id=1, source_target_pairs={{0,2},{2,0},{4,6},{6,4},{8,10},{10,8},{12,14},{14,12},{16,18},{18,... | collective-permute-start | bytes 196616 | tf_op jit(solution)/shard_map/ppermute | solution.py:359
  33.7 5.5 %collective-permute-start.15 = (bf16[256,128]{1,0:T(8,128)(2,1)S(1)}, bf16[256,128]{1,0:T(8,128)(2,1)S(1)}, u32[]{:S(2)}, u32[]{:S(2)}) collective-permute-start(bf16[256,128]{1,0:T(8,128)(2,1)S(1)} %get-tuple-element.35), channel_id=1, source_target_pairs={{0,4},{2,6},{4,0},{6,2},{8,12},{10,14},{12,8},{14,10},{16,20},{18,... | collective-permute-start | bytes 196616 | tf_op jit(solution)/shard_map/ppermute | solution.py:359
  36.4 5.2 %collective-permute-start.16 = (bf16[256,128]{1,0:T(8,128)(2,1)S(1)}, bf16[256,128]{1,0:T(8,128)(2,1)S(1)}, u32[]{:S(2)}, u32[]{:S(2)}) collective-permute-start(bf16[256,128]{1,0:T(8,128)(2,1)S(1)} %get-tuple-element.36), channel_id=1, source_target_pairs={{0,6},{2,4},{4,2},{6,0},{8,14},{10,12},{12,10},{14,8},{16,22},{18,... | collective-permute-start | bytes 196616 | tf_op jit(solution)/shard_map/ppermute | solution.py:359
  36.4 5.2 %collective-permute-start.17 = (bf16[256,128]{1,0:T(8,128)(2,1)S(1)}, bf16[256,128]{1,0:T(8,128)(2,1)S(1)}, u32[]{:S(2)}, u32[]{:S(2)}) collective-permute-start(bf16[256,128]{1,0:T(8,128)(2,1)S(1)} %get-tuple-element.33.refs_0_), channel_id=1, source_target_pairs={{0,1},{1,0},{2,3},{3,2},{4,5},{5,4},{6,7},{7,6},{8,9},{9,8},{10,11... | collective-permute-start | bytes 196616 | tf_op jit(solution)/shard_map/ppermute | solution.py:374
  37.0 4.6 %collective-permute-start.18 = (bf16[256,128]{1,0:T(8,128)(2,1)S(1)}, bf16[256,128]{1,0:T(8,128)(2,1)S(1)}, u32[]{:S(2)}, u32[]{:S(2)}) collective-permute-start(bf16[256,128]{1,0:T(8,128)(2,1)S(1)} %collective-permute-done.14.refs_1_), channel_id=1, source_target_pairs={{0,1},{1,0},{2,3},{3,2},{4,5},{5,4},{6,7},{7,6},{8,9},{9,8},{10,11... | collective-permute-start | bytes 196616 | tf_op jit(solution)/shard_map/ppermute | solution.py:374
  39.2 2.3 %collective-permute-start.19 = (bf16[256,128]{1,0:T(8,128)(2,1)S(1)}, bf16[256,128]{1,0:T(8,128)(2,1)S(1)}, u32[]{:S(2)}, u32[]{:S(2)}) collective-permute-start(bf16[256,128]{1,0:T(8,128)(2,1)S(1)} %collective-permute-done.15.refs_2_), channel_id=1, source_target_pairs={{0,1},{1,0},{2,3},{3,2},{4,5},{5,4},{6,7},{7,6},{8,9},{9,8},{10,11... | collective-permute-start | bytes 196616 | tf_op jit(solution)/shard_map/ppermute | solution.py:374
  41.5 1.3 %collective-permute-start.20 = (bf16[256,128]{1,0:T(8,128)(2,1)S(1)}, bf16[256,128]{1,0:T(8,128)(2,1)S(1)}, u32[]{:S(2)}, u32[]{:S(2)}) collective-permute-start(bf16[256,128]{1,0:T(8,128)(2,1)S(1)} %collective-permute-done.16.refs_3_), channel_id=1, source_target_pairs={{0,1},{1,0},{2,3},{3,2},{4,5},{5,4},{6,7},{7,6},{8,9},{9,8},{10,11... | collective-permute-start | bytes 196616 | tf_op jit(solution)/shard_map/ppermute | solution.py:374
